TPU v7x, 512 devices: a whole 4x4x16 slice. The times are simulated.
512 devices in a mesh: ep: 32 (over z, core), tp: 16 (over y, x).
Axes of the slice: x: 4, y: 4, z: 16, core: 2. Of those that a mesh axis runs over, the one named last changes fastest.
Arguments:
- tokens: bfloat16 [4096, 2048], P('ep'), may hold values from -6 to 6
- routes: int32 [4096, 2], P('ep'), may hold values from 0 to 15, all different within a row; in each aligned block of 128 rows (0 to 127, 128 to 255, ...) at most 18 rows name the same one
- route_weights: float32 [4096, 2], P('ep'), may hold values from 0.2 to 1
- out_grad: bfloat16 [4096, 2048], P('ep'), may hold values from -6 to 6
- gate_proj: bfloat16 [32, 2048, 2048], P('ep', None, 'tp'), may hold values from -0.125 to 0.125
- up_proj: bfloat16 [32, 2048, 2048], P('ep', None, 'tp'), may hold values from -0.125 to 0.125
- down_proj: bfloat16 [32, 2048, 2048], P('ep', 'tp'), may hold values from -0.09375 to 0.09375
Outputs:
- tokens_grad: bfloat16 [4096, 2048], P('ep', 'tp')
- route_grad: float32 [4096, 2], P('ep')
- gate_grad: bfloat16 [32, 2048, 2048], P('ep', None, 'tp')
- up_grad: bfloat16 [32, 2048, 2048], P('ep', None, 'tp')
- down_grad: bfloat16 [32, 2048, 2048], P('ep', 'tp')
Inputs may be any that keep to these rules, and one draw needn't show every extreme that they name: `routes`: each row names 2 different experts. In the rows of one device (an aligned block of 128 rows) no expert is named more than 18 times, and in some blocks one expert is named exactly 18 times.
All inputs are finite; a program needn't handle non-finite values.
Results may differ from a plain program's by a relative error of at most 0.019.
Values may be sent and summed in bfloat16 or wider, within the bound.
No kernel may reach another device: no remote copies, remote signals or barrier semaphores. Data moves between devices by JAX's collectives and lax.ppermute only.
A program may use at most 64 MiB of HBM per device.

v0:
```python
import jax
import jax.numpy as jnp
from jax import lax
from jax.sharding import Mesh
from jax.sharding import PartitionSpec as P

EP = ("ep_0", "ep_1")


def cut_along(array, dim, length):
    before, after = (array.shape[:dim], array.shape[dim + 1 :])
    return jnp.moveaxis(array.reshape(*before, length, -1, *after), dim, 0)


def joined_along(pieces, dim):
    shape = list(pieces.shape[1:])
    shape[dim] *= pieces.shape[0]
    return jnp.moveaxis(pieces, 0, dim).reshape(shape)


def moved_by_axis(pieces, axes, sequence):
    inside = pieces.shape[1:]
    result = pieces.reshape(*(lax.axis_size(a) for a in axes), *inside)
    for k in sequence:
        result = lax.all_to_all(result, axes[k], k, k, tiled=True)
    return result.reshape(-1, *inside)


def two_step_exchange(array, groups, sequence, split_dim, concat_dim):
    length = lax.axis_size(groups[0]) * lax.axis_size(groups[1])
    pieces = cut_along(array, split_dim, length)
    return joined_along(moved_by_axis(pieces, groups, sequence), concat_dim)


def for_sending(array):

    def short(part):
        return part.astype(jnp.bfloat16) if part.dtype == jnp.float32 else part

    return jax.tree.map(short, array)


def partner_2(array, axis, apart):
    return lax.ppermute(array, axis, [(i, i ^ 1 << apart) for i in range(lax.axis_size(axis))])


def side_by_side(arrays, axis, dim, along):
    widths = [a.shape[along] for a in arrays]
    both = jnp.concatenate(arrays, axis=along)
    result = lax.all_gather(both, axis, axis=dim, tiled=True)
    return tuple(jnp.split(result, [sum(widths[:k]) for k in range(1, len(widths))], axis=along))


def sum_at_owner(array, axis, dim):
    length = lax.axis_size(axis)
    pieces = lax.all_to_all(cut_along(array, dim, length), axis, 0, 0, tiled=True)
    return jnp.sum(pieces.astype(jnp.float32), axis=0)


def copy_for_each(array, axis):
    copies = jnp.broadcast_to(array, (lax.axis_size(axis), *array.shape))
    return lax.all_to_all(copies, axis, split_axis=0, concat_axis=0, tiled=True)


def over_copies(array, axis):
    everything = copy_for_each(array, axis)
    return jnp.sum(everything, axis=0)


def slot_rows(routes, expert_count, capacity):
    flat_routes = routes.reshape(-1)
    one_hot = (flat_routes[:, None] == jnp.arange(expert_count, dtype=jnp.int32)[None, :]).astype(
        jnp.int32
    )
    earlier = jnp.cumsum(one_hot, axis=0) - one_hot
    slot_index = jnp.sum(earlier * one_hot, axis=1)
    return flat_routes * capacity + slot_index


def contract_rows(left, right):
    return lax.dot_general(
        left, right, (((0,), (0,)), ((), ())), preferred_element_type=jnp.float32
    )


def contract_cols(left, right):
    return lax.dot_general(
        left, right, (((1,), (1,)), ((), ())), preferred_element_type=jnp.float32
    )


def local(tokens, routes, route_weights, out_grad, gate_proj, up_proj, down_proj):
    ep_size = lax.axis_size(EP)
    expert_count = ep_size // 2
    token_count, model_width = tokens.shape
    top_count = routes.shape[1]
    capacity = 9 * token_count * top_count // (8 * expert_count)
    slot_count = expert_count * capacity
    col_width = model_width // lax.axis_size("tp")
    col_start = lax.axis_index("tp") * col_width
    destination = slot_rows(routes, expert_count, capacity)
    pair_ids = jnp.arange(token_count * top_count, dtype=jnp.int32)
    slot_source = jnp.zeros((slot_count,), jnp.int32).at[destination].set(pair_ids)
    used = jnp.zeros((slot_count,), jnp.bool_).at[destination].set(True)
    token_ids = slot_source // top_count
    token_cols = lax.dynamic_slice_in_dim(tokens, col_start, col_width, 1)
    cot_cols = lax.dynamic_slice_in_dim(out_grad, col_start, col_width, 1)
    token_buf = jnp.where(
        used[:, None], jnp.take(token_cols, token_ids, axis=0), jnp.zeros((), jnp.bfloat16)
    ).reshape(expert_count, capacity, col_width)
    cot_buf = jnp.where(
        used[:, None], jnp.take(cot_cols, token_ids, axis=0), jnp.zeros((), jnp.bfloat16)
    ).reshape(expert_count, capacity, col_width)
    weight_buf = jnp.where(
        used, jnp.take(route_weights.reshape(-1), slot_source, axis=0), 0.0
    ).reshape(expert_count, capacity)
    half_cap = capacity // 2
    received = (
        two_step_exchange(
            token_buf.reshape(ep_size, half_cap, col_width), ("ep_0", "ep_1"), (1, 0), 0, 0
        ),
        two_step_exchange(
            cot_buf.reshape(ep_size, half_cap, col_width), ("ep_0", "ep_1"), (1, 0), 0, 0
        ),
        two_step_exchange(
            weight_buf.reshape(ep_size, half_cap).astype(jnp.bfloat16),
            ("ep_0", "ep_1"),
            (1, 0),
            0,
            0,
        ).astype(jnp.float32),
    )
    parity = lax.axis_index(EP) % 2
    joined = []
    for member in received:
        partner = partner_2(for_sending(member), EP, 0).astype(member.dtype)
        first_half = jnp.where(parity == 0, member, partner)
        second_half = jnp.where(parity == 0, partner, member)
        joined.append(jnp.concatenate([first_half, second_half], axis=1))
    x_part, dy_part, g_rows = joined
    x_rows, dy_rows = side_by_side((x_part, dy_part), "tp", 2, 0)
    row_count = ep_size * capacity
    x_flat = x_rows.reshape(row_count, model_width)
    dy_flat = dy_rows.reshape(row_count, model_width)
    g_flat = g_rows.reshape(row_count, 1)
    gate_local = gate_proj[0]
    up_local = up_proj[0]
    down_local = down_proj[0]
    pre_gate = jnp.dot(x_flat, gate_local, preferred_element_type=jnp.float32)
    pre_up = jnp.dot(x_flat, up_local, preferred_element_type=jnp.float32)
    sigma = jax.nn.sigmoid(pre_gate)
    activ = pre_gate * sigma
    hidden = activ * pre_up
    d_hidden = contract_cols(dy_flat, down_local)
    gate_part = jnp.sum(hidden * d_hidden, axis=1)
    scaled = g_flat * d_hidden
    d_gate = (scaled * pre_up * sigma * (1.0 + pre_gate * (1.0 - sigma))).astype(jnp.bfloat16)
    d_up = (scaled * activ).astype(jnp.bfloat16)
    scaled_cot = (g_flat * dy_flat.astype(jnp.float32)).astype(jnp.bfloat16)
    grad_gate = contract_rows(x_flat, d_gate).astype(jnp.bfloat16)
    grad_up = contract_rows(x_flat, d_up).astype(jnp.bfloat16)
    grad_down = contract_rows(hidden.astype(jnp.bfloat16), scaled_cot).astype(jnp.bfloat16)
    partial_value = contract_cols(d_gate, gate_local) + contract_cols(d_up, up_local)
    summed = sum_at_owner(
        partial_value.reshape(ep_size, capacity, model_width).astype(jnp.bfloat16), "tp", 2
    ).astype(jnp.bfloat16)
    gate_total = over_copies(gate_part.reshape(ep_size, capacity), "tp")
    back_rows, back_gate = (
        lax.all_to_all(summed, EP, split_axis=0, concat_axis=0, tiled=True),
        lax.all_to_all(
            gate_total.astype(jnp.bfloat16), EP, split_axis=0, concat_axis=0, tiled=True
        ).astype(gate_total.dtype),
    )
    col_count = back_rows.shape[2]
    pair_rows = (
        back_rows.astype(jnp.float32)
        .reshape(expert_count, 2, capacity, col_count)
        .sum(axis=1)
        .reshape(slot_count, col_count)
    )
    pair_gate = back_gate.reshape(expert_count, 2, capacity).sum(axis=1).reshape(slot_count)
    tokens_grad = (
        jnp.take(pair_rows, destination, axis=0)
        .reshape(token_count, top_count, col_count)
        .sum(axis=1)
        .astype(jnp.bfloat16)
    )
    route_grad = jnp.take(pair_gate, destination, axis=0).reshape(token_count, top_count)
    return (tokens_grad, route_grad, grad_gate[None], grad_up[None], grad_down[None])


def solution(mesh):
    torus = Mesh(mesh.devices.reshape(16, 2, mesh.shape["tp"]), ("ep_0", "ep_1", "tp"))
    placed = (
        P(EP, None),
        P(EP, None),
        P(EP, None),
        P(EP, None),
        P(EP, None, "tp"),
        P(EP, None, "tp"),
        P(EP, "tp", None),
    )
    return jax.shard_map(
        local,
        mesh=torus,
        in_specs=placed,
        out_specs=(
            P(EP, "tp"),
            P(EP, None),
            P(EP, None, "tp"),
            P(EP, None, "tp"),
            P(EP, "tp", None),
        ),
        check_vma=False,
    )
```

profile of v0, /device:TPU:1, one launch (start us, length us, event | category | flops | bytes accessed | tf_op | source)
XLA Modules:
  0.0 273.0 jit_solution(4949737060180148677)
XLA Ops:
  7.2 0.8 copy.90
  8.3 0.6 reduce-window.6
  9.4 1.4 scatter_custom_fusion.1
  10.8 0.8 constant_dynamic-slice_fusion
  11.6 1.4 gather_fusion.4
  13.0 1.4 gather_fusion.3
  14.4 1.5 scatter_custom_fusion
  16.1 0.7 copy.97
  16.8 10.1 %all-to-all-start.2 = ((bf16[16,2,1,9,128]{4,0,3,2,1:T(8,128)(2,1)}), bf16[16,2,1,9,128]{4,0,3,2,1:T(8,128)(2,1)S(1)}, u32[]{:S(2)}, u32[]{:S(2)}) async-start(bf16[16,2,1,9,128]{4,0,3,2,1:T(8,128)(2,1)} %copy.97), calls=%async_computation.2 | async-start | bytes 147456 | tf_op jit(solution)/shard_map/all_to_all | solution.py:25
  27.0 0.7 copy.100
  28.0 3.6 %all-to-all-start.4 = ((bf16[16,2,1,9,128]{4,0,3,2,1:T(8,128)(2,1)}), bf16[16,2,1,9,128]{4,0,3,2,1:T(8,128)(2,1)S(1)}, u32[]{:S(2)}, u32[]{:S(2)}) async-start(bf16[16,2,1,9,128]{4,0,3,2,1:T(8,128)(2,1)} %copy.100), calls=%async_computation.4 | async-start | bytes 147456 | tf_op jit(solution)/shard_map/all_to_all | solution.py:25
  31.7 0.7 copy.98
  32.3 0.4 all-to-all-done.4
  32.7 9.6 %all-to-all-start.3 = ((bf16[16,2,1,9,128]{4,1,3,2,0:T(2,128)(2,1)}), bf16[16,2,1,9,128]{4,1,3,2,0:T(2,128)(2,1)S(1)}, u32[]{:S(2)}, u32[]{:S(2)}) async-start(bf16[16,2,1,9,128]{4,1,3,2,0:T(2,128)(2,1)} %copy.98), calls=%async_computation.3 | async-start | bytes 147456 | tf_op jit(solution)/shard_map/all_to_all | solution.py:25
  42.3 0.7 copy.101
  43.0 11.0 %all-to-all-done.3 = bf16[16,2,1,9,128]{4,1,3,2,0:T(2,128)(2,1)S(1)} async-done(((bf16[16,2,1,9,128]{4,1,3,2,0:T(2,128)(2,1)}), bf16[16,2,1,9,128]{4,1,3,2,0:T(2,128)(2,1)S(1)}, u32[]{:S(2)}, u32[]{:S(2)}) %all-to-all-start.3) | async-done | bytes 73760 | tf_op jit(solution)/shard_map/all_to_all | solution.py:25
  54.0 4.2 %all-to-all-start.5 = ((bf16[16,2,1,9,128]{4,1,3,2,0:T(2,128)(2,1)}), bf16[16,2,1,9,128]{4,1,3,2,0:T(2,128)(2,1)S(1)}, u32[]{:S(2)}, u32[]{:S(2)}) async-start(bf16[16,2,1,9,128]{4,1,3,2,0:T(2,128)(2,1)} %copy.101), calls=%async_computation.5 | async-start | bytes 147456 | tf_op jit(solution)/shard_map/all_to_all | solution.py:25
  58.3 3.3 %collective-permute-start.1 = (bf16[32,9,128]{2,0,1:T(8,128)(2,1)S(1)}, bf16[32,9,128]{2,0,1:T(8,128)(2,1)S(1)}, u32[]{:S(2)}, u32[]{:S(2)}) collective-permute-start(bf16[32,9,128]{2,0,1:T(8,128)(2,1)S(1)} %bitcast.78), channel_id=1, source_target_pairs={{0,16},{16,0},{32,48},{48,32},{64,80},{80,64},{96,112},{112,96},{1... | collective-permute-start | bytes 221192 | tf_op jit(solution)/shard_map/ppermute | solution.py:44
  61.6 8.3 %all-to-all-done.5 = bf16[16,2,1,9,128]{4,1,3,2,0:T(2,128)(2,1)S(1)} async-done(((bf16[16,2,1,9,128]{4,1,3,2,0:T(2,128)(2,1)}), bf16[16,2,1,9,128]{4,1,3,2,0:T(2,128)(2,1)S(1)}, u32[]{:S(2)}, u32[]{:S(2)}) %all-to-all-start.5) | async-done | bytes 73760 | tf_op jit(solution)/shard_map/all_to_all | solution.py:25
  70.0 4.2 %collective-permute-start.2 = (bf16[32,9,128]{2,0,1:T(8,128)(2,1)S(1)}, bf16[32,9,128]{2,0,1:T(8,128)(2,1)S(1)}, u32[]{:S(2)}, u32[]{:S(2)}) collective-permute-start(bf16[32,9,128]{2,0,1:T(8,128)(2,1)S(1)} %bitcast.80), channel_id=1, source_target_pairs={{0,16},{16,0},{32,48},{48,32},{64,80},{80,64},{96,112},{112,96},{1... | collective-permute-start | bytes 221192 | tf_op jit(solution)/shard_map/ppermute | solution.py:44
  74.2 0.9 collective-permute-done.2
  75.1 0.7 maximum_maximum_fusion
  76.2 2.4 gather_fusion
  78.7 3.7 %all_to_all.51 = bf16[16,2,1,9]{3,0,2,1:T(8,128)(2,1)S(1)} all-to-all(bf16[16,2,1,9]{3,0,2,1:T(8,128)(2,1)S(1)} %copy.95), channel_id=1, replica_groups=mesh['ep_0'=16,'ep_1'=2,'tp'=16] {'ep_1'}, dimensions={1} | all-to-all | bytes 1152 | tf_op jit(solution)/shard_map/all_to_all | solution.py:25
  82.4 14.0 %all_to_all.52 = bf16[16,2,1,9]{3,1,2,0:T(2,128)(2,1)S(1)} all-to-all(bf16[16,2,1,9]{3,1,2,0:T(2,128)(2,1)S(1)} %copy.96), channel_id=1, replica_groups=mesh['ep_0'=16,'ep_1'=2,'tp'=16] {'ep_0'}, dimensions={0} | all-to-all | bytes 1152 | tf_op jit(solution)/shard_map/all_to_all | solution.py:25
  96.4 3.8 %collective-permute-start = (bf16[32,9]{1,0:T(8,128)(2,1)S(1)}, bf16[32,9]{1,0:T(8,128)(2,1)S(1)}, u32[]{:S(2)}, u32[]{:S(2)}) collective-permute-start(bf16[32,9]{1,0:T(8,128)(2,1)S(1)} %bitcast.83), channel_id=1, source_target_pairs={{0,16},{16,0},{32,48},{48,32},{64,80},{80,64},{96,112},{112,96},{1... | collective-permute-start | bytes 1736 | tf_op jit(solution)/shard_map/ppermute | solution.py:44
  100.3 0.6 collective-permute-done
  101.1 40.3 %all-gather.2.cloned.1.call-done = bf16[64,18,2048]{2,0,1:T(8,128)(2,1)} async-done(((bf16[64,18,128]{2,0,1:T(8,128)(2,1)}), bf16[64,18,2048]{2,0,1:T(8,128)(2,1)}) %all-gather.2.cloned.1.call-update) | async-done | bytes 4718608 | tf_op jit(solution)/shard_map/all_gather | solution.py:50
  141.4 2.8 %fusion.28 = (bf16[32,18,2048]{2,0,1:T(8,128)(2,1)S(1)}, bf16[32,18,2048]{2,0,1:T(8,128)(2,1)S(1)}) fusion(bf16[64,18,2048]{2,0,1:T(8,128)(2,1)} %all-gather.2.cloned.1.call-done), kind=kLoop, calls=%fused_computation.81 | loop fusion | bytes 9437184 | tf_op jit(solution)/shard_map/split | solution.py:51
  144.2 3.1 %copy.103 = bf16[32,18,2048]{2,1,0:T(8,128)(2,1)} copy(bf16[32,18,2048]{2,0,1:T(8,128)(2,1)S(1)} %get-tuple-element.40) | data formatting | bytes 4718592 | tf_op jit(solution)/shard_map/split | solution.py:51
  147.2 4.3 %reshape.144 = bf16[576,2048]{1,0:T(8,128)(2,1)} reshape(bf16[32,18,2048]{2,1,0:T(8,128)(2,1)} %copy.103) | data formatting | bytes 4718592 | tf_op jit(solution)/shard_map/reshape | solution.py:144
  151.6 3.1 %copy.104 = bf16[32,18,2048]{2,1,0:T(8,128)(2,1)} copy(bf16[32,18,2048]{2,0,1:T(8,128)(2,1)S(1)} %get-tuple-element.41) | data formatting | bytes 4718592 | tf_op jit(solution)/shard_map/split | solution.py:51
  154.6 2.9 %reshape.145 = bf16[576,2048]{1,0:T(8,128)(2,1)S(1)} reshape(bf16[32,18,2048]{2,1,0:T(8,128)(2,1)} %copy.104) | data formatting | bytes 4718592 | tf_op jit(solution)/shard_map/reshape | solution.py:143
  157.6 0.8 fusion.7
  158.6 0.8 fusion.10
  159.4 1.0 copy-done.1
  160.5 1.5 multiply_reduce_fusion
  162.2 0.7 broadcast_bitcast_fusion
  162.9 1.7 reshape.222
  164.6 4.7 %all-to-all-start.8 = ((f32[16,1,576]{2,1,0:T(1,128)}), f32[16,1,576]{2,1,0:T(1,128)S(1)}, u32[]{:S(2)}, u32[]{:S(2)}) async-start(f32[16,1,576]{2,1,0:T(1,128)} %reshape.222), calls=%async_computation.8 | async-start | bytes 81920 | tf_op jit(solution)/shard_map/all_to_all | solution.py:62
  169.3 1.7 fusion.5
  171.0 0.8 fusion.4
  171.8 0.7 copy.114
  172.5 2.4 copy.117
  174.9 0.8 all-to-all-done.8
  175.7 0.6 copy-done.9
  176.3 5.9 %all-to-all-start.6 = ((bf16[16,32,18,128]{3,1,2,0:T(8,128)(2,1)}), bf16[16,32,18,128]{3,1,2,0:T(8,128)(2,1)}, u32[]{:S(2)}, u32[]{:S(2)}) async-start(bf16[16,32,18,128]{3,1,2,0:T(8,128)(2,1)} %bitcast.75), calls=%async_computation.6 | async-start | bytes 4718592 | tf_op jit(solution)/shard_map/all_to_all | solution.py:56
  182.4 0.5 broadcast.113
  182.9 1.5 reduce.3
  184.5 0.7 copy.110
  185.2 25.5 %all-to-all-done.6 = bf16[16,32,18,128]{3,1,2,0:T(8,128)(2,1)} async-done(((bf16[16,32,18,128]{3,1,2,0:T(8,128)(2,1)}), bf16[16,32,18,128]{3,1,2,0:T(8,128)(2,1)}, u32[]{:S(2)}, u32[]{:S(2)}) %all-to-all-start.6) | async-done | bytes 2359328 | tf_op jit(solution)/shard_map/all_to_all | solution.py:56
  210.7 18.4 %all-to-all-start.9 = ((bf16[32,1,18]{2,1,0:T(2,128)(2,1)}), bf16[32,1,18]{2,1,0:T(2,128)(2,1)S(1)}, u32[]{:S(2)}, u32[]{:S(2)}) async-start(bf16[32,1,18]{2,1,0:T(2,128)(2,1)} %copy.110), calls=%async_computation.9 | async-start | bytes 32768 | tf_op jit(solution)/shard_map/all_to_all | solution.py:170
  229.1 1.7 fusion.1
  230.9 2.0 reduce_sum.73
  232.9 0.8 copy.106
  233.6 7.3 %all-to-all-done.9 = bf16[32,1,18]{2,1,0:T(2,128)(2,1)S(1)} async-done(((bf16[32,1,18]{2,1,0:T(2,128)(2,1)}), bf16[32,1,18]{2,1,0:T(2,128)(2,1)S(1)}, u32[]{:S(2)}, u32[]{:S(2)}) %all-to-all-start.9) | async-done | bytes 1184 | tf_op jit(solution)/shard_map/all_to_all | solution.py:170
  240.9 5.1 %all-to-all-start.7 = ((bf16[32,18,128]{2,1,0:T(8,128)(2,1)}), bf16[32,18,128]{2,1,0:T(8,128)(2,1)S(1)}, u32[]{:S(2)}, u32[]{:S(2)}) async-start(bf16[32,18,128]{2,1,0:T(8,128)(2,1)} %copy.106), calls=%async_computation.7 | async-start | bytes 393216 | tf_op jit(solution)/shard_map/all_to_all | solution.py:169
  246.0 2.8 %fusion.2 = bf16[1,2048,128]{2,1,0:T(8,128)(2,1)} fusion(bf16[576,2048]{1,0:T(8,128)(2,1)S(1)} %reshape.145, bf16[576,128]{1,0:T(8,128)(2,1)} %get-tuple-element.44), kind=kOutput, calls=%fused_computation.15 | convolution fusion | flops 302252032 | bytes 3031040 | tf_op jit(solution)/shard_map/dot_general | solution.py:81
  248.7 2.6 fusion.3
  251.5 1.9 gather_fusion.2
  253.6 0.6 copy.111
  254.2 10.3 %all-to-all-done.7 = bf16[32,18,128]{2,1,0:T(8,128)(2,1)S(1)} async-done(((bf16[32,18,128]{2,1,0:T(8,128)(2,1)}), bf16[32,18,128]{2,1,0:T(8,128)(2,1)S(1)}, u32[]{:S(2)}, u32[]{:S(2)}) %all-to-all-start.7) | async-done | bytes 147488 | tf_op jit(solution)/shard_map/all_to_all | solution.py:169
  264.6 0.7 gather_fusion.1
  265.3 0.9 select_reduce_fusion
  (71 shorter events, 3.3 us)
Async XLA Ops:
  7.2 150.4 %copy-start = (bf16[1,2048,128]{2,1,0:T(8,128)(2,1)S(1)}, bf16[1,2048,128]{2,1,0:T(8,128)(2,1)}, u32[]{:S(2)}) copy-start(bf16[1,2048,128]{2,1,0:T(8,128)(2,1)} %param.13) | copy-start | bytes 1572868
  13.0 62.9 %copy-start.10 = (f32[128,2]{0,1:T(2,128)S(1)}, f32[128,2]{0,1:T(2,128)}, u32[]{:S(2)}) copy-start(f32[128,2]{0,1:T(2,128)} %param.11) | copy-start | bytes 3076
  16.8 11.2 %all-to-all-start.2 = ((bf16[16,2,1,9,128]{4,0,3,2,1:T(8,128)(2,1)}), bf16[16,2,1,9,128]{4,0,3,2,1:T(8,128)(2,1)S(1)}, u32[]{:S(2)}, u32[]{:S(2)}) async-start(bf16[16,2,1,9,128]{4,0,3,2,1:T(8,128)(2,1)} %copy.97), calls=%async_computation.2 | async-start | bytes 147456 | tf_op jit(solution)/shard_map/all_to_all | solution.py:25
  28.0 4.7 %all-to-all-start.4 = ((bf16[16,2,1,9,128]{4,0,3,2,1:T(8,128)(2,1)}), bf16[16,2,1,9,128]{4,0,3,2,1:T(8,128)(2,1)S(1)}, u32[]{:S(2)}, u32[]{:S(2)}) async-start(bf16[16,2,1,9,128]{4,0,3,2,1:T(8,128)(2,1)} %copy.100), calls=%async_computation.4 | async-start | bytes 147456 | tf_op jit(solution)/shard_map/all_to_all | solution.py:25
  32.7 21.3 %all-to-all-start.3 = ((bf16[16,2,1,9,128]{4,1,3,2,0:T(2,128)(2,1)}), bf16[16,2,1,9,128]{4,1,3,2,0:T(2,128)(2,1)S(1)}, u32[]{:S(2)}, u32[]{:S(2)}) async-start(bf16[16,2,1,9,128]{4,1,3,2,0:T(2,128)(2,1)} %copy.98), calls=%async_computation.3 | async-start | bytes 147456 | tf_op jit(solution)/shard_map/all_to_all | solution.py:25
  54.0 15.9 %all-to-all-start.5 = ((bf16[16,2,1,9,128]{4,1,3,2,0:T(2,128)(2,1)}), bf16[16,2,1,9,128]{4,1,3,2,0:T(2,128)(2,1)S(1)}, u32[]{:S(2)}, u32[]{:S(2)}) async-start(bf16[16,2,1,9,128]{4,1,3,2,0:T(2,128)(2,1)} %copy.101), calls=%async_computation.5 | async-start | bytes 147456 | tf_op jit(solution)/shard_map/all_to_all | solution.py:25
  58.2 83.2 %all-gather.2.cloned.1.call-start = ((), (), s32[]{:S(2)}) async-start(), calls=%async_computation.10 | async-start | bytes 5013504 | tf_op jit(solution)/shard_map/all_gather | solution.py:50
  58.3 15.9 %collective-permute-start.1 = (bf16[32,9,128]{2,0,1:T(8,128)(2,1)S(1)}, bf16[32,9,128]{2,0,1:T(8,128)(2,1)S(1)}, u32[]{:S(2)}, u32[]{:S(2)}) collective-permute-start(bf16[32,9,128]{2,0,1:T(8,128)(2,1)S(1)} %bitcast.78), channel_id=1, source_target_pairs={{0,16},{16,0},{32,48},{48,32},{64,80},{80,64},{96,112},{112,96},{1... | collective-permute-start | bytes 221192 | tf_op jit(solution)/shard_map/ppermute | solution.py:44
  70.0 5.1 %collective-permute-start.2 = (bf16[32,9,128]{2,0,1:T(8,128)(2,1)S(1)}, bf16[32,9,128]{2,0,1:T(8,128)(2,1)S(1)}, u32[]{:S(2)}, u32[]{:S(2)}) collective-permute-start(bf16[32,9,128]{2,0,1:T(8,128)(2,1)S(1)} %bitcast.80), channel_id=1, source_target_pairs={{0,16},{16,0},{32,48},{48,32},{64,80},{80,64},{96,112},{112,96},{1... | collective-permute-start | bytes 221192 | tf_op jit(solution)/shard_map/ppermute | solution.py:44
  96.4 4.5 %collective-permute-start = (bf16[32,9]{1,0:T(8,128)(2,1)S(1)}, bf16[32,9]{1,0:T(8,128)(2,1)S(1)}, u32[]{:S(2)}, u32[]{:S(2)}) collective-permute-start(bf16[32,9]{1,0:T(8,128)(2,1)S(1)} %bitcast.83), channel_id=1, source_target_pairs={{0,16},{16,0},{32,48},{48,32},{64,80},{80,64},{96,112},{112,96},{1... | collective-permute-start | bytes 1736 | tf_op jit(solution)/shard_map/ppermute | solution.py:44
  157.6 1.0 copy-start.3
  158.6 0.8 copy-start.4
  158.6 1.8 copy-start.1
  158.6 1.9 copy-start.11
  160.5 1.5 copy-start.6
  164.6 11.1 %all-to-all-start.8 = ((f32[16,1,576]{2,1,0:T(1,128)}), f32[16,1,576]{2,1,0:T(1,128)S(1)}, u32[]{:S(2)}, u32[]{:S(2)}) async-start(f32[16,1,576]{2,1,0:T(1,128)} %reshape.222), calls=%async_computation.8 | async-start | bytes 81920 | tf_op jit(solution)/shard_map/all_to_all | solution.py:62
  169.2 1.7 copy-start.7
  175.7 0.6 copy-start.9
  175.7 53.4 %copy-start.8 = (bf16[576,128]{1,0:T(8,128)(2,1)S(1)}, bf16[576,128]{1,0:T(8,128)(2,1)}, u32[]{:S(2)}) copy-start(bf16[576,128]{1,0:T(8,128)(2,1)} %get-tuple-element.43) | copy-start | bytes 442372
  176.3 34.4 %all-to-all-start.6 = ((bf16[16,32,18,128]{3,1,2,0:T(8,128)(2,1)}), bf16[16,32,18,128]{3,1,2,0:T(8,128)(2,1)}, u32[]{:S(2)}, u32[]{:S(2)}) async-start(bf16[16,32,18,128]{3,1,2,0:T(8,128)(2,1)} %bitcast.75), calls=%async_computation.6 | async-start | bytes 4718592 | tf_op jit(solution)/shard_map/all_to_all | solution.py:56
  210.7 30.2 %all-to-all-start.9 = ((bf16[32,1,18]{2,1,0:T(2,128)(2,1)}), bf16[32,1,18]{2,1,0:T(2,128)(2,1)S(1)}, u32[]{:S(2)}, u32[]{:S(2)}) async-start(bf16[32,1,18]{2,1,0:T(2,128)(2,1)} %copy.110), calls=%async_computation.9 | async-start | bytes 32768 | tf_op jit(solution)/shard_map/all_to_all | solution.py:170
  233.6 15.1 %copy-start.5 = (f32[576,128]{1,0:T(8,128)S(1)}, f32[576,128]{1,0:T(8,128)}, u32[]{:S(2)}) copy-start(f32[576,128]{1,0:T(8,128)} %copy-done.4) | copy-start | bytes 884740
  240.9 23.6 %all-to-all-start.7 = ((bf16[32,18,128]{2,1,0:T(8,128)(2,1)}), bf16[32,18,128]{2,1,0:T(8,128)(2,1)S(1)}, u32[]{:S(2)}, u32[]{:S(2)}) async-start(bf16[32,18,128]{2,1,0:T(8,128)(2,1)} %copy.106), calls=%async_computation.7 | async-start | bytes 393216 | tf_op jit(solution)/shard_map/all_to_all | solution.py:169
  245.9 2.8 %copy-start.2 = (bf16[576,2048]{1,0:T(8,128)(2,1)S(1)}, bf16[576,2048]{1,0:T(8,128)(2,1)}, u32[]{:S(2)}) copy-start(bf16[576,2048]{1,0:T(8,128)(2,1)} %reshape.144) | copy-start | bytes 7077892
Sparse Core Ops, SparseCore 0:
  76.0 65.3 all-gather.1
where the time goes:
time: 274 us; the launch traced here: 273 us
  waiting for transfers between devices  106 us (39%)
  starting transfers between devices  72.8 us (27%)
  local copies, waits for them, and re-layouts  43.2 us (16%)
  blocking collectives  17.7 us (6%)
  between operations  14.5 us (5%)
  matrix products  12.6 us (5%)
  other arithmetic  6.32 us (2%)
    all_gather x1, waiting for transfers between devices, side_by_side(): result = lax.all_gather(both, axis, axis=dim, tiled=True)  40.3 us
    all_to_all x4, starting transfers between devices, moved_by_axis(): result = lax.all_to_all(result, axes[k], k, k, tiled=True)  27.5 us
    all_to_all x1, waiting for transfers between devices, sum_at_owner(): lax.all_to_all(cut_along(array, dim, length), axis, 0, 0, tiled=True)  25.5 us
    all_to_all x4, waiting for transfers between devices, moved_by_axis(): result = lax.all_to_all(result, axes[k], k, k, tiled=True)  20.1 us
    all_to_all x1, starting transfers between devices, local(): lax.all_to_all(gate_total.astype(jnp.bfloat16), EP, split_axis=0, concat_...  18.4 us
    all_to_all x2, blocking collectives, moved_by_axis(): result = lax.all_to_all(result, axes[k], k, k, tiled=True)  17.7 us
    ppermute x3, starting transfers between devices, partner_2(): lax.ppermute(array, axis, [(i, i ^ 1 << apart) for i in range(lax.axis_si...  11.3 us
    all_to_all x1, waiting for transfers between devices, local(): lax.all_to_all(summed, EP, split_axis=0, concat_axis=0, tiled=True)  10.3 us
  transfers between devices with their start and end apart: 12, of which 11 were waited for; matrix products, arithmetic and copies ran while one was open for 10% of the time, Pallas kernels for 0%

commit v1 on v0

v1 whole, which is shorter than its diff:
```python
import jax
import jax.numpy as jnp
from jax import lax
from jax.experimental import pallas as pl
from jax.experimental.pallas import tpu as pltpu
from jax.sharding import Mesh
from jax.sharding import PartitionSpec as P

EP = ("ep_0", "ep_1")
BF = jnp.bfloat16
F32 = jnp.float32

CAP = 18
SRC = 16
HALF_ROWS = SRC * CAP
PIECE = 40
BACK = 24
GATH = 2 * HALF_ROWS + 8
PART = HALF_ROWS + 8


def iota(shape, dim):
    return lax.broadcasted_iota(jnp.int32, shape, dim)


def one_if(cond):
    return jnp.where(cond, 1.0, 0.0).astype(BF)


def split_two(value):
    high = value.astype(BF)
    low = (value - high.astype(F32)).astype(BF)
    return high, low


def contract_cols(left, right):
    return lax.dot_general(left, right, (((1,), (1,)), ((), ())), preferred_element_type=F32)


def matmul(left, right):
    return lax.dot_general(left, right, (((1,), (0,)), ((), ())), preferred_element_type=F32)


def ranks(routes):
    count = routes.shape[0]
    lane = iota((count, 128), 1)
    first = routes[:, 0:1] == lane
    second = routes[:, 1:2] == lane
    member = jnp.where(first | second, 1.0, 0.0)
    before = one_if(iota((count, count), 1) < iota((count, count), 0))
    rank = matmul(before, member.astype(BF))
    return first, second, member, rank


def dispatch_kernel(where_ref, routes_ref, weights_ref, tokens_ref, grad_ref, out_ref):
    first, second, member, rank = ranks(routes_ref[...])
    weights = weights_ref[...]
    weight = jnp.where(first, weights[:, 0:1], 0.0) + jnp.where(second, weights[:, 1:2], 0.0)
    slot = jnp.where(member > 0.0, rank, -100.0)
    slot_t = jnp.transpose(slot)[:16]
    weight_t = jnp.transpose(weight)[:16]
    row = iota((16, PIECE, 128), 1)
    slot_3 = jnp.broadcast_to(slot_t.astype(jnp.int32)[:, None, :], (16, PIECE, 128))
    sel_x = jnp.where(slot_3 == row, 1.0, 0.0)
    sel_dy = jnp.where(slot_3 + CAP == row, 1.0, 0.0)
    chosen = jnp.concatenate(
        [sel_x.reshape(16 * PIECE, 128).astype(BF), sel_dy.reshape(16 * PIECE, 128).astype(BF)], axis=1
    )
    rows = matmul(chosen, jnp.concatenate([tokens_ref[...], grad_ref[...]], axis=0))
    value = jnp.sum(sel_x * weight_t[:, None, :], axis=2, keepdims=True)
    offset = (where_ref[1] % 4) * 32
    spread = jnp.where(iota((16, PIECE, 128), 2) == row + offset, value, 0.0)
    packed = jnp.sum(jnp.where(row < CAP, spread, 0.0), axis=1, keepdims=True)
    high = packed.astype(BF).astype(F32)
    low = packed - high
    rows = rows.reshape(16, PIECE, 128)
    rows = jnp.where(row == 36, high, jnp.where(row == 37, low, rows))
    out_ref[...] = rows.reshape(16 * PIECE, 128).astype(BF)


def copies_kernel(in_ref, out_ref):
    p = iota((2 * HALF_ROWS, 1), 0)
    is_dy = p >= HALF_ROWS
    q = jnp.where(is_dy, p - HALF_ROWS, p)
    source = (q * 3641) >> 16
    target = source * PIECE + (q - source * CAP) + jnp.where(is_dy, CAP, 0)
    pick = one_if(iota((2 * HALF_ROWS, SRC * PIECE), 1) == target)
    col = iota((8, SRC * PIECE), 1)
    of_source = (col * 1639) >> 16
    within = col - of_source * PIECE
    i = iota((8, SRC * PIECE), 0)
    is_low = i >= 4
    group = jnp.where(is_low, i - 4, i)
    pick_w = one_if(((of_source >> 2) == group) & (within == jnp.where(is_low, 37, 36)))
    data = in_ref[...]
    rows = matmul(pick, data).astype(BF)
    extra = matmul(pick_w, data).astype(BF)
    for t in range(16):
        out_ref[t, 0 : 2 * HALF_ROWS, :] = rows
        out_ref[t, 2 * HALF_ROWS : GATH, :] = extra


def lane_of_row():
    r = iota((HALF_ROWS, 1), 0)
    source = (r * 3641) >> 16
    lane = (source & 3) * 32 + (r - source * CAP)
    return source >> 2, lane


def row_weights(extra):
    group, lane = lane_of_row()
    spread = matmul(one_if((iota((HALF_ROWS, 8), 1) & 3) == group), extra)
    return jnp.sum(jnp.where(iota((HALF_ROWS, 128), 1) == lane, spread, 0.0), axis=1, keepdims=True)


def pair_cols(ref, t, start):
    return jnp.concatenate(
        [ref[2 * t, start : start + HALF_ROWS, :], ref[2 * t + 1, start : start + HALF_ROWS, :]], axis=1
    )


def main_kernel(
    own_ref, other_ref, gate_ref, up_ref, down_ref, part_own_ref, part_other_ref, both_ref, hidden_ref
):
    for k, (ref, out_ref) in enumerate(((own_ref, part_own_ref), (other_ref, part_other_ref))):
        pre = jnp.zeros((HALF_ROWS, 256), F32)
        d_hidden = jnp.zeros((HALF_ROWS, 128), F32)
        for t in range(8):
            cols = slice(256 * t, 256 * t + 256)
            proj = jnp.concatenate([gate_ref[cols, :], up_ref[cols, :]], axis=1)
            pre = pre + matmul(pair_cols(ref, t, 0), proj)
            d_hidden = d_hidden + contract_cols(pair_cols(ref, t, HALF_ROWS), down_ref[:, cols])
        pre_gate = pre[:, :128]
        pre_up = pre[:, 128:]
        sigma = jax.nn.sigmoid(pre_gate)
        activ = pre_gate * sigma
        hidden = activ * pre_up
        gate_part = jnp.sum(hidden * d_hidden, axis=1, keepdims=True)
        g = row_weights(ref[0, 2 * HALF_ROWS : GATH, :])
        scaled = g * d_hidden
        d_gate = scaled * pre_up * sigma * (1.0 + pre_gate * (1.0 - sigma))
        d_up = scaled * activ
        both = jnp.concatenate([d_gate.astype(BF), d_up.astype(BF)], axis=1)
        both_ref[k * HALF_ROWS : (k + 1) * HALF_ROWS, :] = both
        hidden_ref[k * HALF_ROWS : (k + 1) * HALF_ROWS, :] = hidden.astype(BF)
        _, lane = lane_of_row()
        spread = jnp.where(iota((HALF_ROWS, 128), 1) == lane, gate_part, 0.0)
        packed = jnp.sum(spread.reshape(4, HALF_ROWS // 4, 128), axis=1)
        extra = jnp.concatenate(split_two(packed), axis=0)
        for t in range(8):
            cols = slice(256 * t, 256 * t + 256)
            proj = jnp.concatenate([gate_ref[cols, :], up_ref[cols, :]], axis=1)
            value = contract_cols(both, proj).astype(BF)
            out_ref[2 * t, 0:HALF_ROWS, :] = value[:, :128]
            out_ref[2 * t + 1, 0:HALF_ROWS, :] = value[:, 128:]
            out_ref[2 * t, HALF_ROWS:PART, :] = extra
            out_ref[2 * t + 1, HALF_ROWS:PART, :] = extra


def weights_kernel(own_ref, other_ref, both_ref, hidden_ref, gate_out, up_out, down_out):
    both_t = jnp.transpose(both_ref[...].astype(F32)).astype(BF)
    hidden_t = jnp.transpose(hidden_ref[...].astype(F32)).astype(BF)
    g_own = row_weights(own_ref[0, 2 * HALF_ROWS : GATH, :])
    g_other = row_weights(other_ref[0, 2 * HALF_ROWS : GATH, :])
    for t in range(8):
        cols = slice(256 * t, 256 * t + 256)
        x = jnp.concatenate([pair_cols(own_ref, t, 0), pair_cols(other_ref, t, 0)], axis=0)
        grads = jnp.transpose(matmul(both_t, x))
        gate_out[cols, :] = grads[:, :128].astype(BF)
        up_out[cols, :] = grads[:, 128:].astype(BF)
        scaled = jnp.concatenate(
            [
                (g_own * pair_cols(own_ref, t, HALF_ROWS).astype(F32)).astype(BF),
                (g_other * pair_cols(other_ref, t, HALF_ROWS).astype(F32)).astype(BF),
            ],
            axis=0,
        )
        down_out[:, cols] = matmul(hidden_t, scaled).astype(BF)


def add_kernel(own_ref, other_ref, out_ref):
    def packed(ref):
        extra = ref[0, HALF_ROWS:PART, :].astype(F32)
        return extra[0:4] + extra[4:8]

    extra = jnp.concatenate(split_two(packed(own_ref) + packed(other_ref)), axis=0)
    for t in range(16):
        rows = own_ref[t, 0:HALF_ROWS, :].astype(F32) + other_ref[t, 0:HALF_ROWS, :].astype(F32)
        out_ref[t, 0:HALF_ROWS, :] = rows.astype(BF)
        out_ref[t, HALF_ROWS:PART, :] = extra


def sum_kernel(in_ref, out_ref):
    rows = in_ref[0, 0:HALF_ROWS, :].astype(F32)
    extra = in_ref[0, HALF_ROWS:PART, :].astype(F32)
    for t in range(1, 16):
        rows = rows + in_ref[t, 0:HALF_ROWS, :].astype(F32)
        extra = extra + in_ref[t, HALF_ROWS:PART, :].astype(F32)
    p = iota((SRC * BACK, 1), 0)
    source = (p * 2731) >> 16
    j = p - source * BACK
    target = jnp.where(j < CAP, source * CAP + j, -1)
    pick = one_if(iota((SRC * BACK, HALF_ROWS), 1) == target)
    col = iota((SRC * BACK, 8), 1)
    group = source >> 2
    pick_g = one_if(((j == 18) & (col == group)) | ((j == 19) & (col == group + 4)))
    packed = jnp.concatenate(split_two(extra[0:4] + extra[4:8]), axis=0)
    out_ref[...] = (matmul(pick, rows.astype(BF)) + matmul(pick_g, packed)).astype(BF)


def combine_kernel(where_ref, routes_ref, in_ref, tokens_ref, route_ref):
    routes = routes_ref[...]
    count = routes.shape[0]
    first, second, member, rank = ranks(routes)
    slot = jnp.where(member > 0.0, rank, -1.0).astype(BF)
    p = iota((1, 16 * BACK), 1)
    expert = (p * 2731) >> 16
    j = p - expert * BACK
    spread = matmul(slot, one_if(iota((128, 16 * BACK), 0) == expert))
    data = in_ref[...]
    tokens_ref[...] = matmul(one_if(spread.astype(jnp.int32) == j), data).astype(BF)
    offset = (where_ref[1] % 4) * 32
    lane = iota((count, 128), 1)
    is_gate = (j == 18) | (j == 19)
    for k, mine in enumerate((first, second)):
        values = matmul(one_if((routes[:, k : k + 1] == expert) & is_gate), data)
        index = jnp.sum(jnp.where(mine, rank, 0.0), axis=1, keepdims=True).astype(jnp.int32)
        route_ref[:, k : k + 1] = jnp.sum(
            jnp.where(lane == index + offset, values, 0.0), axis=1, keepdims=True
        )


def shape(dims, dtype=BF):
    return jax.ShapeDtypeStruct(dims, dtype)


def whole(dims):
    return pl.BlockSpec(dims, lambda i, *_: (0,) * len(dims))


def local(tokens, routes, route_weights, out_grad, gate_proj, up_proj, down_proj):
    count, width = tokens.shape
    where = jnp.stack([lax.axis_index("tp"), lax.axis_index("ep_0")]).astype(jnp.int32)
    columns = pl.BlockSpec((count, 128), lambda i, w: (0, w[0]))
    pieces = pl.pallas_call(
        dispatch_kernel,
        grid_spec=pltpu.PrefetchScalarGridSpec(
            num_scalar_prefetch=1,
            grid=(1,),
            in_specs=[whole(routes.shape), whole(route_weights.shape), columns, columns],
            out_specs=whole((16 * PIECE, 128)),
        ),
        out_shape=shape((16 * PIECE, 128)),
        name="dispatch",
    )(where, routes, route_weights, tokens, out_grad)
    received = lax.all_to_all(pieces.reshape(16, PIECE, 128), "ep_0", 0, 0, tiled=True)
    copies = pl.pallas_call(copies_kernel, out_shape=shape((16, GATH, 128)), name="copies")(
        received.reshape(SRC * PIECE, 128)
    )
    own = lax.all_to_all(copies, "tp", 0, 0, tiled=True)
    swap = [(0, 1), (1, 0)]
    other = lax.ppermute(own, "ep_1", swap)
    gate, up, down = gate_proj[0], up_proj[0], down_proj[0]
    part_own, part_other, both, hidden = pl.pallas_call(
        main_kernel,
        out_shape=(
            shape((16, PART, 128)),
            shape((16, PART, 128)),
            shape((2 * HALF_ROWS, 256)),
            shape((2 * HALF_ROWS, 128)),
        ),
        name="main",
    )(own, other, gate, up, down)
    part_received = lax.ppermute(part_other, "ep_1", swap)
    summed = pl.pallas_call(add_kernel, out_shape=shape((16, PART, 128)), name="add")(
        part_own, part_received
    )
    spread = lax.all_to_all(summed, "tp", 0, 0, tiled=True)
    gate_grad, up_grad, down_grad = pl.pallas_call(
        weights_kernel,
        out_shape=(shape((width, 128)), shape((width, 128)), shape((128, width))),
        name="weights",
    )(own, other, both, hidden)
    back = pl.pallas_call(sum_kernel, out_shape=shape((SRC * BACK, 128)), name="sum")(spread)
    home = lax.all_to_all(back.reshape(SRC, BACK, 128), "ep_0", 0, 0, tiled=True)
    tokens_grad, route_grad = pl.pallas_call(
        combine_kernel,
        grid_spec=pltpu.PrefetchScalarGridSpec(
            num_scalar_prefetch=1,
            grid=(1,),
            in_specs=[whole(routes.shape), whole((16 * BACK, 128))],
            out_specs=(whole((count, 128)), whole(routes.shape)),
        ),
        out_shape=(shape((count, 128)), shape(routes.shape, F32)),
        name="combine",
    )(where, routes, home.reshape(16 * BACK, 128))
    return (tokens_grad, route_grad, gate_grad[None], up_grad[None], down_grad[None])


def solution(mesh):
    torus = Mesh(mesh.devices.reshape(16, 2, mesh.shape["tp"]), ("ep_0", "ep_1", "tp"))
    placed = (
        P(EP, None),
        P(EP, None),
        P(EP, None),
        P(EP, None),
        P(EP, None, "tp"),
        P(EP, None, "tp"),
        P(EP, "tp", None),
    )
    return jax.shard_map(
        local,
        mesh=torus,
        in_specs=placed,
        out_specs=(
            P(EP, "tp"),
            P(EP, None),
            P(EP, None, "tp"),
            P(EP, None, "tp"),
            P(EP, "tp", None),
        ),
        check_vma=False,
    )
```

time: 274 us -> 151 us (0.55)
  waiting for transfers between devices: 106 us -> 13.5 us
  blocking collectives: 17.7 us -> 84.8 us
  starting transfers between devices: 72.8 us -> 17.5 us
  local copies, waits for them, and re-layouts: 43.2 us -> 7.42 us
  Pallas kernels: 0 us -> 25.6 us
  between operations: 14.5 us -> 0.67 us
  matrix products: 12.6 us -> 0 us
  other arithmetic: 6.32 us -> 0.65 us
    all_to_all x2 -> x3, blocking collectives: 17.7 us -> 84.8 us  [the longest x1 33.7 us: local(): own = lax.all_to_all(copies, 'tp', 0, 0, tiled=True)]
    all_to_all x8 -> x1, waiting for transfers between devices: 64 us -> 6.61 us  [local(): lax.all_to_all(back.reshape(SRC, BACK, 128), 'ep_0', 0, 0, tiled=True)]
    all_to_all x8 -> x1, starting transfers between devices: 61.5 us -> 7.55 us  [local(): lax.all_to_all(back.reshape(SRC, BACK, 128), 'ep_0', 0, 0, tiled=True)]
    all_gather x1 -> x0, waiting for transfers between devices: 40.3 us -> none  [side_by_side(): result = lax.all_gather(both, axis, axis=dim, tiled=True)]
    pallas_call x0 -> x7, Pallas kernels: none -> 25.6 us  [the longest x1 6.52 us: local(): pl.pallas_call(main_kernel, out_shape=(shape((16, PART, 128)), shape((16,...]
    dot_general x8 -> x0, matrix products: 12.6 us -> none  [the longest x3 7.07 us: contract_rows(): lax.dot_general(left, right, (((0,), (0,)), ((), ())), preferred_element_...]
    split x3 -> x0, local copies, waits for them, and re-layouts: 8.89 us -> none  [side_by_side(): jnp.split(result, [sum(widths[:k]) for k in range(1, len(widths))], axis=...]
    gather x6 -> x0, local copies, waits for them, and re-layouts: 7.94 us -> none  [the longest x1 2.37 us: local(): jnp.take(route_weights.reshape(-1), slot_source, axis=0)]
  transfers between devices with their start and end apart: 12 -> 3, of which waited for: 11 -> 3; matrix products, arithmetic and copies ran while one was open for 10% -> 0% of each run, Pallas kernels for 0% -> 4%
where the time goes in v1:
time: 151 us; the launch traced here: 150 us
  blocking collectives  84.8 us (56%)
  Pallas kernels  25.6 us (17%)
  starting transfers between devices  17.5 us (12%)
  waiting for transfers between devices  13.5 us (9%)
  local copies, waits for them, and re-layouts  7.42 us (5%)
    all_to_all x1, blocking collectives, local(): own = lax.all_to_all(copies, 'tp', 0, 0, tiled=True)  33.7 us
    all_to_all x1, blocking collectives, local(): lax.all_to_all(pieces.reshape(16, PIECE, 128), 'ep_0', 0, 0, tiled=True)  28 us
    all_to_all x1, blocking collectives, local(): spread = lax.all_to_all(summed, 'tp', 0, 0, tiled=True)  23.1 us
    ppermute x1, starting transfers between devices, local(): other = lax.ppermute(own, 'ep_1', swap)  7.65 us
    all_to_all x1, starting transfers between devices, local(): lax.all_to_all(back.reshape(SRC, BACK, 128), 'ep_0', 0, 0, tiled=True)  7.55 us
    unnamed x11, local copies, waits for them, and re-layouts  7.42 us
    all_to_all x1, waiting for transfers between devices, local(): lax.all_to_all(back.reshape(SRC, BACK, 128), 'ep_0', 0, 0, tiled=True)  6.61 us
    pallas_call x1, Pallas kernels, local(): pl.pallas_call(main_kernel, out_shape=(shape((16, PART, 128)), shape((16,...  6.52 us
  transfers between devices with their start and end apart: 3, of which 3 were waited for; matrix products, arithmetic and copies ran while one was open for 0% of the time, Pallas kernels for 4%

profile of v1, /device:TPU:1, one launch (start us, length us, event | category | flops | bytes accessed | tf_op | source)
XLA Modules:
  0.0 150.1 jit_solution(8939849878522999883)
XLA Ops:
  0.6 1.4 copy.14.routes_ref
  2.0 1.4 copy.13.weights_ref
  3.5 0.7 pad_add_fusion.where_ref
  4.1 2.8 %dispatch.1 = bf16[640,128]{1,0:T(8,128)(2,1)} custom-call(s32[2]{0:T(128)} %pad_add_fusion.where_ref, s32[128,2]{1,0:T(8,128)} %copy.14.routes_ref, f32[128,2]{1,0:T(8,128)} %copy.13.weights_ref, bf16[128,2048]{1,0:T(8,128)(2,1)} %tokens_ref.1, bf16[128,2048]{1,0:T(8,128)(2,1)} %grad_ref.1), custom_call_target="tpu_custom_call" | custom-call | tf_op jit(solution)/shard_map/dispatch/pallas_call | solution.py:245
  6.9 28.0 %all_to_all.20 = bf16[16,40,128]{2,1,0:T(8,128)(2,1)} all-to-all(bf16[16,40,128]{2,1,0:T(8,128)(2,1)} %bitcast.13), channel_id=1, replica_groups=mesh['ep_0'=16,'ep_1'=2,'tp'=16] {'ep_0'}, dimensions={0} | all-to-all | bytes 327680 | tf_op jit(solution)/shard_map/all_to_all | solution.py:256
  34.9 2.8 %copies.1 = bf16[16,584,128]{2,1,0:T(8,128)(2,1)} custom-call(bf16[640,128]{1,0:T(8,128)(2,1)} %bitcast.12), custom_call_target="tpu_custom_call" | custom-call | tf_op jit(solution)/shard_map/copies/pallas_call | solution.py:257
  37.7 33.7 %all_to_all.21.own_ref = bf16[16,584,128]{2,1,0:T(8,128)(2,1)S(1)} all-to-all(bf16[16,584,128]{2,1,0:T(8,128)(2,1)} %copies.1), channel_id=1, replica_groups=mesh['ep_0'=16,'ep_1'=2,'tp'=16] {'tp'}, dimensions={0} | all-to-all | bytes 4784128 | tf_op jit(solution)/shard_map/all_to_all | solution.py:260
  71.4 0.0 copy-start
  71.4 7.6 %collective-permute-start = (bf16[16,584,128]{2,1,0:T(8,128)(2,1)S(1)}, bf16[16,584,128]{2,1,0:T(8,128)(2,1)S(1)}, u32[]{:S(2)}, u32[]{:S(2)}) collective-permute-start(bf16[16,584,128]{2,1,0:T(8,128)(2,1)S(1)} %all_to_all.21.own_ref), channel_id=1, source_target_pairs={{0,16},{16,0},{1,17},{17,1},{2,18},{18,2},{3,19},{19,3},{4,20},{20... | collective-permute-start | bytes 7176200 | tf_op jit(solution)/shard_map/ppermute | solution.py:262
  79.0 4.2 %collective-permute-done.other_ref = bf16[16,584,128]{2,1,0:T(8,128)(2,1)S(1)} collective-permute-done((bf16[16,584,128]{2,1,0:T(8,128)(2,1)S(1)}, bf16[16,584,128]{2,1,0:T(8,128)(2,1)S(1)}, u32[]{:S(2)}, u32[]{:S(2)}) %collective-permute-start) | collective-permute-done | bytes 2392096 | tf_op jit(solution)/shard_map/ppermute | solution.py:262
  83.2 0.0 copy-start.1
  83.2 1.4 copy-done.1
  84.6 0.0 copy-done
  84.6 6.5 %main.1 = (bf16[16,296,128]{2,1,0:T(8,128)(2,1)}, bf16[16,296,128]{2,1,0:T(8,128)(2,1)}, bf16[576,256]{1,0:T(8,128)(2,1)}, bf16[576,128]{1,0:T(8,128)(2,1)}) custom-call(bf16[16,584,128]{2,1,0:T(8,128)(2,1)} %copy-done, bf16[16,584,128]{2,1,0:T(8,128)(2,1)} %copy-done.1, bf16[2048,128]{1,0:T(8,128)(2,1)} %bitcast.14, bf16[2048,128]{1,0:T(8,128)(2,1)} %bitcast.15, ...), custom_call_target="tpu_custom_call" | custom-call | tf_op jit(solution)/shard_map/main/pallas_call | solution.py:264
  91.2 2.3 %collective-permute-start.1 = (bf16[16,296,128]{2,1,0:T(8,128)(2,1)}, bf16[16,296,128]{2,1,0:T(8,128)(2,1)S(1)}, u32[]{:S(2)}, u32[]{:S(2)}) collective-permute-start(bf16[16,296,128]{2,1,0:T(8,128)(2,1)} %get-tuple-element.15), channel_id=1, source_target_pairs={{0,16},{16,0},{1,17},{17,1},{2,18},{18,2},{3,19},{19,3},{4,20},{20... | collective-permute-start | bytes 3637256 | tf_op jit(solution)/shard_map/ppermute | solution.py:274
  93.5 2.7 %collective-permute-done.1.other_ref = bf16[16,296,128]{2,1,0:T(8,128)(2,1)S(1)} collective-permute-done((bf16[16,296,128]{2,1,0:T(8,128)(2,1)}, bf16[16,296,128]{2,1,0:T(8,128)(2,1)S(1)}, u32[]{:S(2)}, u32[]{:S(2)}) %collective-permute-start.1) | collective-permute-done | bytes 1212448 | tf_op jit(solution)/shard_map/ppermute | solution.py:274
  96.2 0.0 copy-start.2
  96.2 1.1 copy-done.2
  97.2 3.0 %add.3 = bf16[16,296,128]{2,1,0:T(8,128)(2,1)} custom-call(bf16[16,296,128]{2,1,0:T(8,128)(2,1)} %get-tuple-element.14.own_ref, bf16[16,296,128]{2,1,0:T(8,128)(2,1)} %copy-done.2), custom_call_target="tpu_custom_call" | custom-call | tf_op jit(solution)/shard_map/add/pallas_call | solution.py:275
  100.2 23.1 %all_to_all.22.in_ref = bf16[16,296,128]{2,1,0:T(8,128)(2,1)} all-to-all(bf16[16,296,128]{2,1,0:T(8,128)(2,1)} %add.3), channel_id=1, replica_groups=mesh['ep_0'=16,'ep_1'=2,'tp'=16] {'tp'}, dimensions={0} | all-to-all | bytes 2424832 | tf_op jit(solution)/shard_map/all_to_all | solution.py:278
  123.3 2.4 %sum.1 = bf16[384,128]{1,0:T(8,128)(2,1)} custom-call(bf16[16,296,128]{2,1,0:T(8,128)(2,1)} %all_to_all.22.in_ref), custom_call_target="tpu_custom_call" | custom-call | tf_op jit(solution)/shard_map/sum/pallas_call | solution.py:284
  125.6 7.5 %all-to-all-start.3 = ((bf16[16,24,128]{2,1,0:T(8,128)(2,1)}), bf16[16,24,128]{2,1,0:T(8,128)(2,1)S(1)}, u32[]{:S(2)}, u32[]{:S(2)}) async-start(bf16[16,24,128]{2,1,0:T(8,128)(2,1)} %bitcast.18), calls=%async_computation.3 | async-start | bytes 196608 | tf_op jit(solution)/shard_map/all_to_all | solution.py:285
  133.2 5.3 %weights.1 = (bf16[2048,128]{1,0:T(8,128)(2,1)}, bf16[2048,128]{1,0:T(8,128)(2,1)}, bf16[128,2048]{1,0:T(8,128)(2,1)}) custom-call(bf16[16,584,128]{2,1,0:T(8,128)(2,1)} %copy-done, bf16[16,584,128]{2,1,0:T(8,128)(2,1)} %copy-done.1, bf16[576,256]{1,0:T(8,128)(2,1)} %get-tuple-element.18.both_ref, bf16[576,128]{1,0:T(8,128)(2,1)} %get-tuple-element.19.hidden_ref), custom_call_target="tpu_custom_call" | custom-call | tf_op jit(solution)/shard_map/weights/pallas_call | solution.py:279
  138.5 6.6 %all-to-all-done.3 = bf16[16,24,128]{2,1,0:T(8,128)(2,1)S(1)} async-done(((bf16[16,24,128]{2,1,0:T(8,128)(2,1)}), bf16[16,24,128]{2,1,0:T(8,128)(2,1)S(1)}, u32[]{:S(2)}, u32[]{:S(2)}) %all-to-all-start.3) | async-done | bytes 98336 | tf_op jit(solution)/shard_map/all_to_all | solution.py:285
  145.1 0.0 copy-start.3
  145.1 0.6 copy-done.3
  145.7 2.9 %combine.1 = (bf16[128,128]{1,0:T(8,128)(2,1)}, f32[128,2]{1,0:T(8,128)}) custom-call(s32[2]{0:T(128)} %pad_add_fusion.where_ref, s32[128,2]{1,0:T(8,128)} %copy.14.routes_ref, bf16[384,128]{1,0:T(8,128)(2,1)} %bitcast.17), custom_call_target="tpu_custom_call" | custom-call | tf_op jit(solution)/shard_map/combine/pallas_call | solution.py:286
  148.6 1.5 copy.15
Async XLA Ops:
  71.4 13.3 %copy-start = (bf16[16,584,128]{2,1,0:T(8,128)(2,1)}, bf16[16,584,128]{2,1,0:T(8,128)(2,1)S(1)}, u32[]{:S(2)}) copy-start(bf16[16,584,128]{2,1,0:T(8,128)(2,1)S(1)} %all_to_all.21.own_ref) | copy-start | bytes 7176196
  71.4 11.8 %collective-permute-start = (bf16[16,584,128]{2,1,0:T(8,128)(2,1)S(1)}, bf16[16,584,128]{2,1,0:T(8,128)(2,1)S(1)}, u32[]{:S(2)}, u32[]{:S(2)}) collective-permute-start(bf16[16,584,128]{2,1,0:T(8,128)(2,1)S(1)} %all_to_all.21.own_ref), channel_id=1, source_target_pairs={{0,16},{16,0},{1,17},{17,1},{2,18},{18,2},{3,19},{19,3},{4,20},{20... | collective-permute-start | bytes 7176200 | tf_op jit(solution)/shard_map/ppermute | solution.py:262
  83.2 1.4 copy-start.1
  91.2 5.0 %collective-permute-start.1 = (bf16[16,296,128]{2,1,0:T(8,128)(2,1)}, bf16[16,296,128]{2,1,0:T(8,128)(2,1)S(1)}, u32[]{:S(2)}, u32[]{:S(2)}) collective-permute-start(bf16[16,296,128]{2,1,0:T(8,128)(2,1)} %get-tuple-element.15), channel_id=1, source_target_pairs={{0,16},{16,0},{1,17},{17,1},{2,18},{18,2},{3,19},{19,3},{4,20},{20... | collective-permute-start | bytes 3637256 | tf_op jit(solution)/shard_map/ppermute | solution.py:274
  96.2 1.1 copy-start.2
  125.6 19.5 %all-to-all-start.3 = ((bf16[16,24,128]{2,1,0:T(8,128)(2,1)}), bf16[16,24,128]{2,1,0:T(8,128)(2,1)S(1)}, u32[]{:S(2)}, u32[]{:S(2)}) async-start(bf16[16,24,128]{2,1,0:T(8,128)(2,1)} %bitcast.18), calls=%async_computation.3 | async-start | bytes 196608 | tf_op jit(solution)/shard_map/all_to_all | solution.py:285
  145.1 0.6 copy-start.3

commit v2 on v1

v2 whole, which is shorter than its diff:
```python
import jax
import jax.numpy as jnp
from jax import lax
from jax.experimental import pallas as pl
from jax.experimental.pallas import tpu as pltpu
from jax.sharding import Mesh
from jax.sharding import PartitionSpec as P


EP = ("ep_0", "ep_1")
BF = jnp.bfloat16
F32 = jnp.float32

CAP = 18
SRC = 16
ROWS = SRC * CAP
PIECE = 40
BACK = 24
GATH = 2 * ROWS + 8
LIMIT = pltpu.CompilerParams(vmem_limit_bytes=24 * 1024 * 1024)
PART = ROWS + 8


def iota(shape, dim):
    return lax.broadcasted_iota(jnp.int32, shape, dim)


def one_if(cond):
    return jnp.where(cond, 1.0, 0.0).astype(BF)


def split_two(value):
    high = value.astype(BF)
    low = (value - high.astype(F32)).astype(BF)
    return high, low


def contract_cols(left, right):
    return lax.dot_general(left, right, (((1,), (1,)), ((), ())), preferred_element_type=F32)


def matmul(left, right):
    return lax.dot_general(left, right, (((1,), (0,)), ((), ())), preferred_element_type=F32)


def ranks(routes):
    count = routes.shape[1]
    expert = iota((16, count), 0)
    first = routes[0:1, :] == expert
    second = routes[1:2, :] == expert
    member = jnp.where(first | second, 1.0, 0.0)
    before = one_if(iota((count, count), 0) < iota((count, count), 1))
    rank = matmul(member.astype(BF), before)
    return first, second, member, rank


def dispatch_kernel(routes_ref, weights_ref, tokens_ref, grad_ref, out_ref, data_ref, sems):
    start = pl.multiple_of(lax.axis_index("tp") * 128, 128)
    loads = [
        pltpu.make_async_copy(
            ref.at[:, pl.ds(start, 128)], data_ref.at[pl.ds(128 * k, 128), :], sems.at[k]
        )
        for k, ref in enumerate((tokens_ref, grad_ref))
    ]
    for load in loads:
        load.start()
    first, second, member, rank = ranks(routes_ref[...])
    weights = weights_ref[...]
    weight = jnp.where(first, weights[0:1, :], 0.0) + jnp.where(second, weights[1:2, :], 0.0)
    slot = jnp.where(member > 0.0, rank, -100.0).astype(jnp.int32)
    row = iota((16, PIECE, 128), 1)
    slot_3 = jnp.broadcast_to(slot[:, None, :], (16, PIECE, 128))
    sel_x = jnp.where(slot_3 == row, 1.0, 0.0)
    sel_dy = jnp.where(slot_3 + CAP == row, 1.0, 0.0)
    chosen = jnp.concatenate(
        [sel_x.reshape(16 * PIECE, 128).astype(BF), sel_dy.reshape(16 * PIECE, 128).astype(BF)], axis=1
    )
    value = jnp.sum(sel_x * weight[:, None, :], axis=2, keepdims=True)
    offset = (lax.axis_index("ep_0") % 4) * 32
    spread = jnp.where(iota((16, PIECE, 128), 2) == row + offset, value, 0.0)
    packed = jnp.sum(jnp.where(row < CAP, spread, 0.0), axis=1, keepdims=True)
    high = packed.astype(BF).astype(F32)
    low = packed - high
    for load in loads:
        load.wait()
    rows = matmul(chosen, data_ref[...]).reshape(16, PIECE, 128)
    rows = jnp.where(row == 36, high, jnp.where(row == 37, low, rows))
    out_ref[...] = rows.reshape(16 * PIECE, 128).astype(BF)


def plan_kernel(routes_ref, copies_ref, back_ref, combine_ref, lanes_ref):
    p = iota((2 * ROWS, 1), 0)
    is_dy = p >= ROWS
    q = jnp.where(is_dy, p - ROWS, p)
    source = (q * 3641) >> 16
    target = source * PIECE + (q - source * CAP) + jnp.where(is_dy, CAP, 0)
    copies_ref[0 : 2 * ROWS, :] = one_if(iota((2 * ROWS, SRC * PIECE), 1) == target)
    col = iota((16, SRC * PIECE), 1)
    of_source = (col * 1639) >> 16
    within = col - of_source * PIECE
    i = iota((16, SRC * PIECE), 0)
    pick = ((of_source >> 2) == (i & 3)) & (within == jnp.where(i >= 4, 37, 36)) & (i < 8)
    copies_ref[2 * ROWS : 2 * ROWS + 16, :] = one_if(pick)

    p = iota((SRC * BACK, 1), 0)
    source = (p * 2731) >> 16
    j = p - source * BACK
    target = jnp.where(j < CAP, source * CAP + j, -1)
    target = jnp.where(j == 18, ROWS + (source >> 2), target)
    target = jnp.where(j == 19, ROWS + 4 + (source >> 2), target)
    back_ref[...] = one_if(iota((SRC * BACK, PART), 1) == target)

    routes = routes_ref[...]
    first, second, member, rank = ranks(routes)
    slot = jnp.where(member > 0.0, rank, -100.0).astype(jnp.int32)
    row = iota((16, BACK, 128), 1)
    sel = jnp.where(jnp.broadcast_to(slot[:, None, :], (16, BACK, 128)) == row, 1.0, 0.0)
    combine_ref[0:128, :] = jnp.transpose(sel.reshape(16 * BACK, 128)).astype(BF)
    offset = (lax.axis_index("ep_0") % 4) * 32
    is_gate = (row == 18) | (row == 19)
    for k, mine in enumerate((first, second)):
        chosen = jnp.where(mine, 1.0, 0.0)[:, None, :]
        sel = jnp.where(is_gate, jnp.broadcast_to(chosen, (16, BACK, 128)), 0.0)
        combine_ref[128 * (k + 1) : 128 * (k + 2), :] = jnp.transpose(
            sel.reshape(16 * BACK, 128)
        ).astype(BF)
        index = jnp.sum(jnp.where(mine, rank, 0.0), axis=0, keepdims=True).astype(jnp.int32)
        lanes = jnp.where(iota((128, 128), 0) == index + offset, 1.0, 0.0)
        lanes_ref[128 * k : 128 * (k + 1), :] = jnp.transpose(lanes).astype(BF)


def copies_kernel(in_ref, pick_ref, out_ref):
    rows = matmul(pick_ref[...], in_ref[...]).astype(BF)
    for t in range(16):
        out_ref[t] = rows[:GATH]


def lane_of_row():
    r = iota((ROWS, 1), 0)
    source = (r * 3641) >> 16
    lane = (source & 3) * 32 + (r - source * CAP)
    return source >> 2, lane


def row_weights(extra):
    group, lane = lane_of_row()
    spread = matmul(one_if((iota((ROWS, 8), 1) & 3) == group), extra)
    return jnp.sum(jnp.where(iota((ROWS, 128), 1) == lane, spread, 0.0), axis=1, keepdims=True)


def pair_cols(ref, t, start):
    return jnp.concatenate([ref[2 * t, start : start + ROWS, :], ref[2 * t + 1, start : start + ROWS, :]], axis=1)


def main_kernel(own_ref, *refs):
    weights, (part_out, both_ref, hidden_ref) = refs[:6], refs[6:9]
    held, (part_ref, both_held, hidden_held), (in_sems, out_sems) = refs[9:15], refs[15:18], refs[18:20]
    loads = []
    for s in range(4):
        stage = []
        for k in range(6):
            part = pl.ds(512 * s, 512)
            index = (slice(None), part) if k % 3 == 2 else (part, slice(None))
            stage.append(
                pltpu.make_async_copy(weights[k].at[index], held[k].at[index], in_sems.at[6 * s + k])
            )
            stage[-1].start()
        loads.append(stage)
    gate, up, down, gate_2, up_2, down_2 = held
    pre_gate = jnp.zeros((ROWS, 256), F32)
    pre_up = jnp.zeros((ROWS, 256), F32)
    d_hidden = jnp.zeros((ROWS, 256), F32)
    for t in range(8):
        if t % 2 == 0:
            for load in loads[t // 2]:
                load.wait()
        cols = slice(256 * t, 256 * t + 256)
        x = pair_cols(own_ref, t, 0)
        pre_gate = pre_gate + matmul(x, jnp.concatenate([gate[cols, :], gate_2[cols, :]], axis=1))
        pre_up = pre_up + matmul(x, jnp.concatenate([up[cols, :], up_2[cols, :]], axis=1))
        d_hidden = d_hidden + contract_cols(
            pair_cols(own_ref, t, ROWS), jnp.concatenate([down[:, cols], down_2[:, cols]], axis=0)
        )
    sigma = jax.nn.sigmoid(pre_gate)
    activ = pre_gate * sigma
    hidden = activ * pre_up
    gate_part = jnp.sum(hidden * d_hidden, axis=1, keepdims=True)
    scaled = row_weights(own_ref[0, 2 * ROWS : GATH, :]) * d_hidden
    d_gate = (scaled * pre_up * sigma * (1.0 + pre_gate * (1.0 - sigma))).astype(BF)
    d_up = (scaled * activ).astype(BF)
    both_held[:, 0:256] = d_gate
    both_held[:, 256:512] = d_up
    hidden_held[...] = hidden.astype(BF)
    stores = [
        pltpu.make_async_copy(both_held, both_ref, out_sems.at[0]),
        pltpu.make_async_copy(hidden_held, hidden_ref, out_sems.at[1]),
    ]
    for store in stores:
        store.start()
    _, lane = lane_of_row()
    spread = jnp.where(iota((ROWS, 128), 1) == lane, gate_part, 0.0)
    packed = jnp.sum(spread.reshape(4, ROWS // 4, 128), axis=1)
    extra = jnp.concatenate(split_two(packed), axis=0)
    for t in range(8):
        cols = slice(256 * t, 256 * t + 256)
        value = contract_cols(d_gate, jnp.concatenate([gate[cols, :], gate_2[cols, :]], axis=1))
        value = value + contract_cols(d_up, jnp.concatenate([up[cols, :], up_2[cols, :]], axis=1))
        value = value.astype(BF)
        for k in range(2):
            part_ref[2 * t + k, 0:ROWS, :] = value[:, 128 * k : 128 * k + 128]
            part_ref[2 * t + k, ROWS:PART, :] = extra
        two = pl.ds(2 * t, 2)
        stores.append(pltpu.make_async_copy(part_ref.at[two], part_out.at[two], out_sems.at[2 + t]))
        stores[-1].start()
    for store in stores:
        store.wait()


def half_grads(own_ref, both_ref, hidden_ref, half):
    lanes = slice(128 * half, 128 * half + 128)
    late = slice(256 + 128 * half, 256 + 128 * half + 128)
    both = jnp.concatenate([both_ref[:, lanes], both_ref[:, late]], axis=1)
    both_t = jnp.transpose(both.astype(F32)).astype(BF)
    hidden_t = jnp.transpose(hidden_ref[:, lanes].astype(F32)).astype(BF)
    g = row_weights(own_ref[0, 2 * ROWS : GATH, :])
    for t in range(8):
        cols = slice(256 * t, 256 * t + 256)
        scaled = (g * pair_cols(own_ref, t, ROWS).astype(F32)).astype(BF)
        yield cols, matmul(both_t, pair_cols(own_ref, t, 0)), matmul(hidden_t, scaled)


def partner_grads_kernel(own_ref, both_ref, hidden_ref, out_ref):
    for cols, both, down in half_grads(own_ref, both_ref, hidden_ref, 1):
        out_ref[0:256, cols] = both.astype(BF)
        out_ref[256:384, cols] = down.astype(BF)


def own_grads_kernel(own_ref, both_ref, hidden_ref, other_ref, gate_out, up_out, down_out):
    for cols, both, down in half_grads(own_ref, both_ref, hidden_ref, 0):
        grads = jnp.transpose(both + other_ref[0:256, cols].astype(F32))
        gate_out[cols, :] = grads[:, :128].astype(BF)
        up_out[cols, :] = grads[:, 128:].astype(BF)
        down_out[:, cols] = (down + other_ref[256:384, cols].astype(F32)).astype(BF)


def sum_kernel(in_ref, pick_ref, out_ref):
    rows = in_ref[0].astype(F32)
    for t in range(1, 16):
        rows = rows + in_ref[t].astype(F32)
    packed = rows[ROWS : ROWS + 4] + rows[ROWS + 4 : PART]
    high = packed.astype(BF).astype(F32)
    rows = jnp.concatenate([rows[:ROWS], high, packed - high], axis=0).astype(BF)
    out_ref[...] = matmul(pick_ref[...], rows).astype(BF)


def combine_kernel(in_ref, pick_ref, lanes_ref, tokens_ref, route_ref):
    values = matmul(pick_ref[...], in_ref[...])
    tokens_ref[...] = values[:128].astype(BF)
    gates = lax.dot_general(
        jnp.ones((8, 128), F32),
        values[128:] * lanes_ref[...].astype(F32),
        (((1,), (1,)), ((), ())),
        precision=lax.Precision.HIGHEST,
        preferred_element_type=F32,
    )
    route_ref[0:1, :] = gates[0:1, :128]
    route_ref[1:2, :] = gates[0:1, 128:]


def shape(dims, dtype=BF):
    return jax.ShapeDtypeStruct(dims, dtype)


def far_shape(dims, dtype=BF):
    return pltpu.HBM(dims, dtype)


def near(dims, dtype=BF):
    return pltpu.VMEM(dims, dtype)


def far(value):
    return pltpu.with_memory_space_constraint(value, pltpu.HBM)


def hold(value):
    return pltpu.with_memory_space_constraint(value, pltpu.VMEM)


def local(tokens, routes, route_weights, out_grad, gate_proj, up_proj, down_proj):
    return steps(tokens, routes, route_weights, out_grad, gate_proj[0], up_proj[0], down_proj[0])


def exchange(value, axis):
    return lax.all_to_all(value, axis, 0, 0, tiled=True)


def to_partner(value):
    return lax.ppermute(value, "ep_1", [(0, 1), (1, 0)])


def kernel(body, **settings):
    return pl.pallas_call(body, compiler_params=LIMIT, **settings)


def steps(tokens, routes, route_weights, out_grad, gate, up, down):
    count, width = tokens.shape
    routes_t = routes.T
    weights_t = route_weights.T
    vmem = pl.BlockSpec(memory_space=pltpu.VMEM)
    hbm = pl.BlockSpec(memory_space=pltpu.HBM)
    pieces = kernel(
        dispatch_kernel,
        in_specs=[vmem, vmem, hbm, hbm],
        out_shape=near((16 * PIECE, 128)),
        scratch_shapes=[pltpu.VMEM((256, 128), BF), pltpu.SemaphoreType.DMA((2,))],
    )(routes_t, weights_t, far(tokens), far(out_grad))
    received = exchange(pieces.reshape(16, PIECE, 128), "ep_0")
    gate_2, up_2, down_2 = (to_partner(w) for w in (gate, up, down))
    pick_copies, pick_back, pick_combine, lanes = kernel(
        plan_kernel,
        out_shape=(
            near((2 * ROWS + 16, SRC * PIECE)),
            shape((SRC * BACK, PART)),
            shape((384, 16 * BACK)),
            shape((256, 128)),
        ),
    )(routes_t)
    received, gate_2, up_2, down_2 = lax.optimization_barrier((received, gate_2, up_2, down_2))
    copies = kernel(copies_kernel, out_shape=near((16, GATH, 128)))(
        hold(received.reshape(SRC * PIECE, 128)), hold(pick_copies)
    )
    own = exchange(copies, "tp")
    part, both, hidden = kernel(
        main_kernel,
        in_specs=[vmem] + [hbm] * 6,
        out_specs=(hbm, hbm, hbm),
        out_shape=(far_shape((16, PART, 128)), far_shape((ROWS, 512)), far_shape((ROWS, 256))),
        scratch_shapes=[
            *[pltpu.VMEM(w.shape, BF) for w in (gate, up, down, gate, up, down)],
            pltpu.VMEM((16, PART, 128), BF),
            pltpu.VMEM((ROWS, 512), BF),
            pltpu.VMEM((ROWS, 256), BF),
            pltpu.SemaphoreType.DMA((24,)),
            pltpu.SemaphoreType.DMA((10,)),
        ],
    )(hold(own), *(far(w) for w in (gate, up, down, gate_2, up_2, down_2)))
    spread = exchange(part, "tp")
    partner = kernel(partner_grads_kernel, out_shape=shape((384, width)))(own, both, hidden)
    mine = to_partner(partner)
    gate_grad, up_grad, down_grad = kernel(
        own_grads_kernel, out_shape=(shape((width, 128)), shape((width, 128)), shape((128, width)))
    )(own, both, hidden, mine)
    back = kernel(sum_kernel, out_shape=near((SRC * BACK, 128)))(hold(spread), hold(pick_back))
    home = exchange(back.reshape(SRC, BACK, 128), "ep_0")
    tokens_grad, route_grad = kernel(
        combine_kernel, out_shape=(shape((count, 128)), shape((2, count), F32))
    )(hold(home.reshape(16 * BACK, 128)), hold(pick_combine), hold(lanes))
    return (tokens_grad, route_grad.T, gate_grad[None], up_grad[None], down_grad[None])


def solution(mesh):
    torus = Mesh(mesh.devices.reshape(16, 2, mesh.shape["tp"]), ("ep_0", "ep_1", "tp"))
    placed = (
        P(EP, None),
        P(EP, None),
        P(EP, None),
        P(EP, None),
        P(EP, None, "tp"),
        P(EP, None, "tp"),
        P(EP, "tp", None),
    )
    return jax.shard_map(
        local,
        mesh=torus,
        in_specs=placed,
        out_specs=(
            P(EP, "tp"),
            P(EP, None),
            P(EP, None, "tp"),
            P(EP, None, "tp"),
            P(EP, "tp", None),
        ),
        check_vma=False,
    )
```

time: 151 us -> 128 us (0.85)
  starting transfers between devices: 17.5 us -> 30.6 us
  Pallas kernels: 25.6 us -> 12.7 us
  waiting for transfers between devices: 13.5 us -> 3.44 us
  blocking collectives: 84.8 us -> 75.3 us
  local copies, waits for them, and re-layouts: 7.42 us -> 3.92 us
    pallas_call x7 -> x8, Pallas kernels: 25.6 us -> 12.7 us  [the longest x1 4.69 us: steps(): kernel(main_kernel, in_specs=[vmem] + [hbm] * 6, out_specs=(hbm, hbm, hbm...]
    all_to_all x3, blocking collectives: 84.8 us -> 75.3 us  [exchange(): return lax.all_to_all(value, axis, 0, 0, tiled=True)]
    all_to_all x1, starting transfers between devices: 7.55 us -> 15.7 us  [exchange(): return lax.all_to_all(value, axis, 0, 0, tiled=True)]
    ppermute x2 -> x4, waiting for transfers between devices: 6.9 us -> 0.23 us  [to_partner(): return lax.ppermute(value, 'ep_1', [(0, 1), (1, 0)])]
    ppermute x2 -> x4, starting transfers between devices: 9.93 us -> 14.8 us  [to_partner(): return lax.ppermute(value, 'ep_1', [(0, 1), (1, 0)])]
    unnamed x11 -> x22, local copies, waits for them, and re-layouts: 7.42 us -> 3.92 us
    all_to_all x1, waiting for transfers between devices: 6.61 us -> 3.21 us  [exchange(): return lax.all_to_all(value, axis, 0, 0, tiled=True)]
  transfers between devices with their start and end apart: 3 -> 5, of which waited for: 3 -> 2; matrix products, arithmetic and copies ran while one was open for 0% -> 0% of each run, Pallas kernels for 4% -> 2%
where the time goes in v2:
time: 128 us; the launch traced here: 127 us
  blocking collectives  75.3 us (59%)
  starting transfers between devices  30.6 us (24%)
  Pallas kernels  12.7 us (10%)
  local copies, waits for them, and re-layouts  3.92 us (3%)
  waiting for transfers between devices  3.44 us (3%)
    all_to_all x3, blocking collectives, exchange(): return lax.all_to_all(value, axis, 0, 0, tiled=True)  75.3 us
    all_to_all x1, starting transfers between devices, exchange(): return lax.all_to_all(value, axis, 0, 0, tiled=True)  15.7 us
    ppermute x4, starting transfers between devices, to_partner(): return lax.ppermute(value, 'ep_1', [(0, 1), (1, 0)])  14.8 us
    pallas_call x1, Pallas kernels, steps(): kernel(main_kernel, in_specs=[vmem] + [hbm] * 6, out_specs=(hbm, hbm, hbm...  4.69 us
    unnamed x22, local copies, waits for them, and re-layouts  3.92 us
    all_to_all x1, waiting for transfers between devices, exchange(): return lax.all_to_all(value, axis, 0, 0, tiled=True)  3.21 us
  transfers between devices with their start and end apart: 5, of which 2 were waited for; matrix products, arithmetic and copies ran while one was open for 0% of the time, Pallas kernels for 2%

profile of v2, /device:TPU:1, one launch (start us, length us, event | category | flops | bytes accessed | tf_op | source)
XLA Modules:
  0.0 126.8 jit_solution(11168663299784822190)
XLA Ops:
  0.6 0.0 copy-start.4
  0.6 0.7 copy-done.4
  1.3 0.0 copy-start.5
  1.3 0.7 copy-done.5
  2.0 1.7 %shard_map.110 = bf16[640,128]{1,0:T(8,128)(2,1)} custom-call(s32[2,128]{1,0:T(2,128)S(1)} %bitcast.17, f32[2,128]{1,0:T(2,128)S(1)} %bitcast.16, bf16[128,2048]{1,0:T(8,128)(2,1)} %tokens_ref.1, bf16[128,2048]{1,0:T(8,128)(2,1)} %grad_ref.1), custom_call_target="tpu_custom_call" | custom-call | tf_op jit(solution)/shard_map/pallas_call | solution.py:312
  3.7 15.7 %all-to-all-start = ((bf16[16,40,128]{2,1,0:T(8,128)(2,1)}), bf16[16,40,128]{2,1,0:T(8,128)(2,1)S(1)}, u32[]{:S(2)}, u32[]{:S(2)}) async-start(bf16[16,40,128]{2,1,0:T(8,128)(2,1)} %bitcast.2), calls=%async_computation | async-start | bytes 327680 | tf_op jit(solution)/shard_map/all_to_all | solution.py:295
  19.5 2.9 %collective-permute-start = (bf16[2048,128]{1,0:T(8,128)(2,1)}, bf16[2048,128]{1,0:T(8,128)(2,1)S(1)}, u32[]{:S(2)}, u32[]{:S(2)}) collective-permute-start(bf16[2048,128]{1,0:T(8,128)(2,1)} %bitcast.19), channel_id=1, source_target_pairs={{0,16},{16,0},{1,17},{17,1},{2,18},{18,2},{3,19},{19,3},{4,20},{20... | collective-permute-start | bytes 1572872 | tf_op jit(solution)/shard_map/ppermute | solution.py:299
  22.3 1.9 %collective-permute-start.1 = (bf16[2048,128]{1,0:T(8,128)(2,1)}, bf16[2048,128]{1,0:T(8,128)(2,1)S(1)}, u32[]{:S(2)}, u32[]{:S(2)}) collective-permute-start(bf16[2048,128]{1,0:T(8,128)(2,1)} %bitcast.21), channel_id=1, source_target_pairs={{0,16},{16,0},{1,17},{17,1},{2,18},{18,2},{3,19},{19,3},{4,20},{20... | collective-permute-start | bytes 1572872 | tf_op jit(solution)/shard_map/ppermute | solution.py:299
  24.3 2.4 %collective-permute-start.2 = (bf16[128,2048]{1,0:T(8,128)(2,1)}, bf16[128,2048]{1,0:T(8,128)(2,1)S(1)}, u32[]{:S(2)}, u32[]{:S(2)}) collective-permute-start(bf16[128,2048]{1,0:T(8,128)(2,1)} %bitcast.23), channel_id=1, source_target_pairs={{0,16},{16,0},{1,17},{17,1},{2,18},{18,2},{3,19},{19,3},{4,20},{20... | collective-permute-start | bytes 1572872 | tf_op jit(solution)/shard_map/ppermute | solution.py:299
  26.7 0.0 copy-start.6
  26.7 0.7 copy-done.6
  27.4 0.8 shard_map.111
  28.1 0.0 collective-permute-done.refs_3_
  28.2 0.0 copy-start.8
  28.2 0.0 collective-permute-done.1.refs_4_
  28.2 0.0 copy-start.9
  28.2 0.2 collective-permute-done.2.refs_5_
  28.4 0.0 copy-start.10
  28.4 3.2 %all-to-all-done = bf16[16,40,128]{2,1,0:T(8,128)(2,1)S(1)} async-done(((bf16[16,40,128]{2,1,0:T(8,128)(2,1)}), bf16[16,40,128]{2,1,0:T(8,128)(2,1)S(1)}, u32[]{:S(2)}, u32[]{:S(2)}) %all-to-all-start) | async-done | bytes 163872 | tf_op jit(solution)/shard_map/all_to_all | solution.py:295
  31.6 0.4 shard_map.112
  32.0 0.0 copy-done.8
  32.1 0.0 copy-done.9
  32.1 0.0 copy-done.10
  32.1 33.5 %all_to_all.20.own_ref = bf16[16,584,128]{2,1,0:T(8,128)(2,1)S(1)} all-to-all(bf16[16,584,128]{2,1,0:T(8,128)(2,1)S(1)} %shard_map.112), channel_id=1, replica_groups=mesh['ep_0'=16,'ep_1'=2,'tp'=16] {'tp'}, dimensions={0} | all-to-all | bytes 4784128 | tf_op jit(solution)/shard_map/all_to_all | solution.py:295
  65.6 4.7 %shard_map.113 = (bf16[16,296,128]{2,1,0:T(8,128)(2,1)}, bf16[288,512]{1,0:T(8,128)(2,1)}, bf16[288,256]{1,0:T(8,128)(2,1)}) custom-call(bf16[16,584,128]{2,1,0:T(8,128)(2,1)S(1)} %all_to_all.20.own_ref, bf16[2048,128]{1,0:T(8,128)(2,1)} %bitcast.20, bf16[2048,128]{1,0:T(8,128)(2,1)} %bitcast.22, bf16[128,2048]{1,0:T(8,128)(2,1)} %bitcast.24, ...), custom_call_target="tpu_custom_call" | custom-call | tf_op jit(solution)/shard_map/pallas_call | solution.py:334
  70.3 0.0 copy-start
  70.3 1.0 copy-done
  71.3 0.0 copy-start.2
  71.3 0.9 copy-done.2
  72.2 0.0 copy-start.7
  72.2 1.3 %shard_map.116 = bf16[384,2048]{1,0:T(8,128)(2,1)S(1)} custom-call(bf16[16,584,128]{2,1,0:T(8,128)(2,1)S(1)} %all_to_all.20.own_ref, bf16[288,512]{1,0:T(8,128)(2,1)S(1)} %copy-done, bf16[288,256]{1,0:T(8,128)(2,1)S(1)} %copy-done.2), custom_call_target="tpu_custom_call" | custom-call | tf_op jit(solution)/shard_map/pallas_call | solution.py:349
  73.5 7.6 %collective-permute-start.3 = (bf16[384,2048]{1,0:T(8,128)(2,1)S(1)}, bf16[384,2048]{1,0:T(8,128)(2,1)S(1)}, u32[]{:S(2)}, u32[]{:S(2)}) collective-permute-start(bf16[384,2048]{1,0:T(8,128)(2,1)S(1)} %shard_map.116), channel_id=1, source_target_pairs={{0,16},{16,0},{1,17},{17,1},{2,18},{18,2},{3,19},{19,3},{4,20},{20... | collective-permute-start | bytes 4718600 | tf_op jit(solution)/shard_map/ppermute | solution.py:299
  81.1 0.0 copy-done.7
  81.1 21.4 %all_to_all.21.in_ref = bf16[16,296,128]{2,1,0:T(8,128)(2,1)S(1)} all-to-all(bf16[16,296,128]{2,1,0:T(8,128)(2,1)S(1)} %copy-done.7), channel_id=1, replica_groups=mesh['ep_0'=16,'ep_1'=2,'tp'=16] {'tp'}, dimensions={0} | all-to-all | bytes 2424832 | tf_op jit(solution)/shard_map/all_to_all | solution.py:295
  102.5 0.0 copy-start.1
  102.5 0.0 copy-start.3
  102.5 0.4 shard_map.114
  102.8 20.4 %all_to_all.22 = bf16[16,24,128]{2,1,0:T(8,128)(2,1)S(1)} all-to-all(bf16[16,24,128]{2,1,0:T(8,128)(2,1)S(1)} %bitcast.15), channel_id=1, replica_groups=mesh['ep_0'=16,'ep_1'=2,'tp'=16] {'ep_0'}, dimensions={0} | all-to-all | bytes 196608 | tf_op jit(solution)/shard_map/all_to_all | solution.py:295
  123.3 1.1 shard_map.115
  124.4 0.0 collective-permute-done.3.other_ref
  124.4 0.0 copy-done.1
  124.4 0.0 copy-done.3
  124.4 2.4 %shard_map.117 = (bf16[2048,128]{1,0:T(8,128)(2,1)}, bf16[2048,128]{1,0:T(8,128)(2,1)}, bf16[128,2048]{1,0:T(8,128)(2,1)}) custom-call(bf16[16,584,128]{2,1,0:T(8,128)(2,1)S(1)} %all_to_all.20.own_ref, bf16[288,512]{1,0:T(8,128)(2,1)S(1)} %copy-done.1, bf16[288,256]{1,0:T(8,128)(2,1)S(1)} %copy-done.3, bf16[384,2048]{1,0:T(8,128)(2,1)S(1)} %collective-permute-done.3.other_ref), custom_call_target="tpu_custom_call" | custom-call | tf_op jit(solution)/shard_map/pallas_call | solution.py:351
Async XLA Ops:
  0.6 0.7 copy-start.4
  1.3 0.7 copy-start.5
  3.7 27.9 %all-to-all-start = ((bf16[16,40,128]{2,1,0:T(8,128)(2,1)}), bf16[16,40,128]{2,1,0:T(8,128)(2,1)S(1)}, u32[]{:S(2)}, u32[]{:S(2)}) async-start(bf16[16,40,128]{2,1,0:T(8,128)(2,1)} %bitcast.2), calls=%async_computation | async-start | bytes 327680 | tf_op jit(solution)/shard_map/all_to_all | solution.py:295
  19.5 8.7 %collective-permute-start = (bf16[2048,128]{1,0:T(8,128)(2,1)}, bf16[2048,128]{1,0:T(8,128)(2,1)S(1)}, u32[]{:S(2)}, u32[]{:S(2)}) collective-permute-start(bf16[2048,128]{1,0:T(8,128)(2,1)} %bitcast.19), channel_id=1, source_target_pairs={{0,16},{16,0},{1,17},{17,1},{2,18},{18,2},{3,19},{19,3},{4,20},{20... | collective-permute-start | bytes 1572872 | tf_op jit(solution)/shard_map/ppermute | solution.py:299
  22.3 5.8 %collective-permute-start.1 = (bf16[2048,128]{1,0:T(8,128)(2,1)}, bf16[2048,128]{1,0:T(8,128)(2,1)S(1)}, u32[]{:S(2)}, u32[]{:S(2)}) collective-permute-start(bf16[2048,128]{1,0:T(8,128)(2,1)} %bitcast.21), channel_id=1, source_target_pairs={{0,16},{16,0},{1,17},{17,1},{2,18},{18,2},{3,19},{19,3},{4,20},{20... | collective-permute-start | bytes 1572872 | tf_op jit(solution)/shard_map/ppermute | solution.py:299
  24.3 4.1 %collective-permute-start.2 = (bf16[128,2048]{1,0:T(8,128)(2,1)}, bf16[128,2048]{1,0:T(8,128)(2,1)S(1)}, u32[]{:S(2)}, u32[]{:S(2)}) collective-permute-start(bf16[128,2048]{1,0:T(8,128)(2,1)} %bitcast.23), channel_id=1, source_target_pairs={{0,16},{16,0},{1,17},{17,1},{2,18},{18,2},{3,19},{19,3},{4,20},{20... | collective-permute-start | bytes 1572872 | tf_op jit(solution)/shard_map/ppermute | solution.py:299
  26.7 0.7 copy-start.6
  28.2 3.9 %copy-start.8 = (bf16[2048,128]{1,0:T(8,128)(2,1)}, bf16[2048,128]{1,0:T(8,128)(2,1)S(1)}, u32[]{:S(2)}) copy-start(bf16[2048,128]{1,0:T(8,128)(2,1)S(1)} %collective-permute-done.refs_3_) | copy-start | bytes 1572868
  28.2 3.9 %copy-start.9 = (bf16[2048,128]{1,0:T(8,128)(2,1)}, bf16[2048,128]{1,0:T(8,128)(2,1)S(1)}, u32[]{:S(2)}) copy-start(bf16[2048,128]{1,0:T(8,128)(2,1)S(1)} %collective-permute-done.1.refs_4_) | copy-start | bytes 1572868
  28.4 3.6 %copy-start.10 = (bf16[128,2048]{1,0:T(8,128)(2,1)}, bf16[128,2048]{1,0:T(8,128)(2,1)S(1)}, u32[]{:S(2)}) copy-start(bf16[128,2048]{1,0:T(8,128)(2,1)S(1)} %collective-permute-done.2.refs_5_) | copy-start | bytes 1572868
  70.3 1.0 copy-start
  71.3 0.9 copy-start.2
  72.2 8.9 %copy-start.7 = (bf16[16,296,128]{2,1,0:T(8,128)(2,1)S(1)}, bf16[16,296,128]{2,1,0:T(8,128)(2,1)}, u32[]{:S(2)}) copy-start(bf16[16,296,128]{2,1,0:T(8,128)(2,1)} %get-tuple-element.26) | copy-start | bytes 3637252
  73.5 50.9 %collective-permute-start.3 = (bf16[384,2048]{1,0:T(8,128)(2,1)S(1)}, bf16[384,2048]{1,0:T(8,128)(2,1)S(1)}, u32[]{:S(2)}, u32[]{:S(2)}) collective-permute-start(bf16[384,2048]{1,0:T(8,128)(2,1)S(1)} %shard_map.116), channel_id=1, source_target_pairs={{0,16},{16,0},{1,17},{17,1},{2,18},{18,2},{3,19},{19,3},{4,20},{20... | collective-permute-start | bytes 4718600 | tf_op jit(solution)/shard_map/ppermute | solution.py:299
  102.5 21.9 %copy-start.1 = (bf16[288,512]{1,0:T(8,128)(2,1)S(1)}, bf16[288,512]{1,0:T(8,128)(2,1)}, u32[]{:S(2)}) copy-start(bf16[288,512]{1,0:T(8,128)(2,1)} %get-tuple-element.32.both_ref) | copy-start | bytes 884740
  102.5 21.9 %copy-start.3 = (bf16[288,256]{1,0:T(8,128)(2,1)S(1)}, bf16[288,256]{1,0:T(8,128)(2,1)}, u32[]{:S(2)}) copy-start(bf16[288,256]{1,0:T(8,128)(2,1)} %get-tuple-element.33.hidden_ref) | copy-start | bytes 442372

commit v3 on v2

--- a/solution.py
+++ b/solution.py
@@ -54,16 +54,24 @@
     return first, second, member, rank
 
 
-def dispatch_kernel(routes_ref, weights_ref, tokens_ref, grad_ref, out_ref, data_ref, sems):
+def dispatch_kernel(
+    routes_hbm, weights_hbm, tokens_ref, grad_ref, out_ref, data_ref, routes_ref, weights_ref, sems
+):
     start = pl.multiple_of(lax.axis_index("tp") * 128, 128)
+    small = [
+        pltpu.make_async_copy(routes_hbm, routes_ref, sems.at[2]),
+        pltpu.make_async_copy(weights_hbm, weights_ref, sems.at[3]),
+    ]
     loads = [
         pltpu.make_async_copy(
             ref.at[:, pl.ds(start, 128)], data_ref.at[pl.ds(128 * k, 128), :], sems.at[k]
         )
         for k, ref in enumerate((tokens_ref, grad_ref))
     ]
-    for load in loads:
+    for load in small + loads:
         load.start()
+    for load in small:
+        load.wait()
     first, second, member, rank = ranks(routes_ref[...])
     weights = weights_ref[...]
     weight = jnp.where(first, weights[0:1, :], 0.0) + jnp.where(second, weights[1:2, :], 0.0)
@@ -88,7 +96,22 @@
     out_ref[...] = rows.reshape(16 * PIECE, 128).astype(BF)
 
 
-def plan_kernel(routes_ref, copies_ref, back_ref, combine_ref, lanes_ref):
+def plan_kernel(
+    routes_hbm, gate, up, down, copies_ref, back_ref, combine_ref, lanes_ref, swap_ref, routes_ref, sems
+):
+    routes_load = pltpu.make_async_copy(routes_hbm, routes_ref, sems.at[18])
+    routes_load.start()
+    moves = [
+        pltpu.make_async_copy(ref, swap_ref.at[pl.ds(2048 * k, 2048), :], sems.at[16 + k])
+        for k, ref in enumerate((gate, up))
+    ] + [
+        pltpu.make_async_copy(
+            down.at[:, pl.ds(128 * t, 128)], swap_ref.at[pl.ds(4096 + 128 * t, 128), :], sems.at[t]
+        )
+        for t in range(16)
+    ]
+    for move in moves:
+        move.start()
     p = iota((2 * ROWS, 1), 0)
     is_dy = p >= ROWS
     q = jnp.where(is_dy, p - ROWS, p)
@@ -110,6 +133,7 @@
     target = jnp.where(j == 19, ROWS + 4 + (source >> 2), target)
     back_ref[...] = one_if(iota((SRC * BACK, PART), 1) == target)
 
+    routes_load.wait()
     routes = routes_ref[...]
     first, second, member, rank = ranks(routes)
     slot = jnp.where(member > 0.0, rank, -100.0).astype(jnp.int32)
@@ -127,6 +151,8 @@
         index = jnp.sum(jnp.where(mine, rank, 0.0), axis=0, keepdims=True).astype(jnp.int32)
         lanes = jnp.where(iota((128, 128), 0) == index + offset, 1.0, 0.0)
         lanes_ref[128 * k : 128 * (k + 1), :] = jnp.transpose(lanes).astype(BF)
+    for move in moves:
+        move.wait()
 
 
 def copies_kernel(in_ref, pick_ref, out_ref):
@@ -152,34 +178,24 @@
     return jnp.concatenate([ref[2 * t, start : start + ROWS, :], ref[2 * t + 1, start : start + ROWS, :]], axis=1)
 
 
-def main_kernel(own_ref, *refs):
-    weights, (part_out, both_ref, hidden_ref) = refs[:6], refs[6:9]
-    held, (part_ref, both_held, hidden_held), (in_sems, out_sems) = refs[9:15], refs[15:18], refs[18:20]
-    loads = []
-    for s in range(4):
-        stage = []
-        for k in range(6):
-            part = pl.ds(512 * s, 512)
-            index = (slice(None), part) if k % 3 == 2 else (part, slice(None))
-            stage.append(
-                pltpu.make_async_copy(weights[k].at[index], held[k].at[index], in_sems.at[6 * s + k])
-            )
-            stage[-1].start()
-        loads.append(stage)
-    gate, up, down, gate_2, up_2, down_2 = held
+def main_kernel(own_ref, gate, up, down, swap_ref, part_ref, both_ref, hidden_ref):
     pre_gate = jnp.zeros((ROWS, 256), F32)
     pre_up = jnp.zeros((ROWS, 256), F32)
     d_hidden = jnp.zeros((ROWS, 256), F32)
+
+    def both_halves(ref, t, first):
+        cols = slice(256 * t, 256 * t + 256)
+        return jnp.concatenate([ref[cols, :], swap_ref[first + 256 * t : first + 256 * t + 256, :]], axis=1)
+
     for t in range(8):
-        if t % 2 == 0:
-            for load in loads[t // 2]:
-                load.wait()
-        cols = slice(256 * t, 256 * t + 256)
         x = pair_cols(own_ref, t, 0)
-        pre_gate = pre_gate + matmul(x, jnp.concatenate([gate[cols, :], gate_2[cols, :]], axis=1))
-        pre_up = pre_up + matmul(x, jnp.concatenate([up[cols, :], up_2[cols, :]], axis=1))
+        pre_gate = pre_gate + matmul(x, both_halves(gate, t, 0))
+        pre_up = pre_up + matmul(x, both_halves(up, t, 2048))
+        at = 4096 + 256 * t
+        down_2 = jnp.concatenate([swap_ref[at : at + 128, :], swap_ref[at + 128 : at + 256, :]], axis=1)
         d_hidden = d_hidden + contract_cols(
-            pair_cols(own_ref, t, ROWS), jnp.concatenate([down[:, cols], down_2[:, cols]], axis=0)
+            pair_cols(own_ref, t, ROWS),
+            jnp.concatenate([down[:, 256 * t : 256 * t + 256], down_2], axis=0),
         )
     sigma = jax.nn.sigmoid(pre_gate)
     activ = pre_gate * sigma
@@ -188,32 +204,20 @@
     scaled = row_weights(own_ref[0, 2 * ROWS : GATH, :]) * d_hidden
     d_gate = (scaled * pre_up * sigma * (1.0 + pre_gate * (1.0 - sigma))).astype(BF)
     d_up = (scaled * activ).astype(BF)
-    both_held[:, 0:256] = d_gate
-    both_held[:, 256:512] = d_up
-    hidden_held[...] = hidden.astype(BF)
-    stores = [
-        pltpu.make_async_copy(both_held, both_ref, out_sems.at[0]),
-        pltpu.make_async_copy(hidden_held, hidden_ref, out_sems.at[1]),
-    ]
-    for store in stores:
-        store.start()
+    both_ref[:, 0:256] = d_gate
+    both_ref[:, 256:512] = d_up
+    hidden_ref[...] = hidden.astype(BF)
     _, lane = lane_of_row()
     spread = jnp.where(iota((ROWS, 128), 1) == lane, gate_part, 0.0)
     packed = jnp.sum(spread.reshape(4, ROWS // 4, 128), axis=1)
     extra = jnp.concatenate(split_two(packed), axis=0)
     for t in range(8):
-        cols = slice(256 * t, 256 * t + 256)
-        value = contract_cols(d_gate, jnp.concatenate([gate[cols, :], gate_2[cols, :]], axis=1))
-        value = value + contract_cols(d_up, jnp.concatenate([up[cols, :], up_2[cols, :]], axis=1))
+        value = contract_cols(d_gate, both_halves(gate, t, 0))
+        value = value + contract_cols(d_up, both_halves(up, t, 2048))
         value = value.astype(BF)
         for k in range(2):
             part_ref[2 * t + k, 0:ROWS, :] = value[:, 128 * k : 128 * k + 128]
             part_ref[2 * t + k, ROWS:PART, :] = extra
-        two = pl.ds(2 * t, 2)
-        stores.append(pltpu.make_async_copy(part_ref.at[two], part_out.at[two], out_sems.at[2 + t]))
-        stores[-1].start()
-    for store in stores:
-        store.wait()
 
 
 def half_grads(own_ref, both_ref, hidden_ref, half):
@@ -309,42 +313,39 @@
     weights_t = route_weights.T
     vmem = pl.BlockSpec(memory_space=pltpu.VMEM)
     hbm = pl.BlockSpec(memory_space=pltpu.HBM)
+    small = [pltpu.VMEM((2, count), jnp.int32), pltpu.VMEM((2, count), F32)]
     pieces = kernel(
         dispatch_kernel,
-        in_specs=[vmem, vmem, hbm, hbm],
+        in_specs=[hbm] * 4,
         out_shape=near((16 * PIECE, 128)),
-        scratch_shapes=[pltpu.VMEM((256, 128), BF), pltpu.SemaphoreType.DMA((2,))],
-    )(routes_t, weights_t, far(tokens), far(out_grad))
+        scratch_shapes=[pltpu.VMEM((256, 128), BF), *small, pltpu.SemaphoreType.DMA((4,))],
+    )(far(routes_t), far(weights_t), far(tokens), far(out_grad))
     received = exchange(pieces.reshape(16, PIECE, 128), "ep_0")
-    gate_2, up_2, down_2 = (to_partner(w) for w in (gate, up, down))
-    pick_copies, pick_back, pick_combine, lanes = kernel(
+    pick_copies, pick_back, pick_combine, lanes, packed = kernel(
         plan_kernel,
+        in_specs=[hbm] * 4,
+        out_specs=(vmem, vmem, vmem, vmem, hbm),
         out_shape=(
             near((2 * ROWS + 16, SRC * PIECE)),
             shape((SRC * BACK, PART)),
             shape((384, 16 * BACK)),
             shape((256, 128)),
+            far_shape((3 * width, 128)),
         ),
-    )(routes_t)
-    received, gate_2, up_2, down_2 = lax.optimization_barrier((received, gate_2, up_2, down_2))
+        scratch_shapes=[small[0], pltpu.SemaphoreType.DMA((19,))],
+    )(far(routes_t), far(gate), far(up), far(down))
+    packed_2 = to_partner(packed)
+    received, packed_2 = lax.optimization_barrier((received, packed_2))
     copies = kernel(copies_kernel, out_shape=near((16, GATH, 128)))(
         hold(received.reshape(SRC * PIECE, 128)), hold(pick_copies)
     )
-    own = exchange(copies, "tp")
+    own = hold(exchange(copies, "tp"))
     part, both, hidden = kernel(
         main_kernel,
-        in_specs=[vmem] + [hbm] * 6,
-        out_specs=(hbm, hbm, hbm),
-        out_shape=(far_shape((16, PART, 128)), far_shape((ROWS, 512)), far_shape((ROWS, 256))),
-        scratch_shapes=[
-            *[pltpu.VMEM(w.shape, BF) for w in (gate, up, down, gate, up, down)],
-            pltpu.VMEM((16, PART, 128), BF),
-            pltpu.VMEM((ROWS, 512), BF),
-            pltpu.VMEM((ROWS, 256), BF),
-            pltpu.SemaphoreType.DMA((24,)),
-            pltpu.SemaphoreType.DMA((10,)),
-        ],
-    )(hold(own), *(far(w) for w in (gate, up, down, gate_2, up_2, down_2)))
+        in_specs=[vmem] * 5,
+        out_specs=(vmem, vmem, vmem),
+        out_shape=(near((16, PART, 128)), near((ROWS, 512)), near((ROWS, 256))),
+    )(own, gate, up, down, hold(packed_2))
     spread = exchange(part, "tp")
     partner = kernel(partner_grads_kernel, out_shape=shape((384, width)))(own, both, hidden)
     mine = to_partner(partner)

time: 128 us -> 172 us (1.34)
  Pallas kernels: 12.7 us -> 58.2 us
  blocking collectives: 75.3 us -> 98.6 us
  starting transfers between devices: 30.6 us -> 13.7 us
  local copies, waits for them, and re-layouts: 3.92 us -> 0.02 us
  waiting for transfers between devices: 3.44 us -> 0.01 us
    pallas_call x3, Pallas kernels: 7.18 us -> 52.6 us  [the longest x1 48.9 us: steps(): kernel(plan_kernel, in_specs=[hbm] * 4, out_specs=(vmem, vmem, vmem, vmem...]
    all_to_all x3 -> x4, blocking collectives: 75.3 us -> 98.6 us  [exchange(): return lax.all_to_all(value, axis, 0, 0, tiled=True)]
    all_to_all x1 -> x0, starting transfers between devices: 15.7 us -> none  [exchange(): return lax.all_to_all(value, axis, 0, 0, tiled=True)]
    unnamed x22 -> x6, local copies, waits for them, and re-layouts: 3.92 us -> 0.02 us
    all_to_all x1 -> x0, waiting for transfers between devices: 3.21 us -> none  [exchange(): return lax.all_to_all(value, axis, 0, 0, tiled=True)]
    ppermute x4 -> x2, starting transfers between devices: 14.8 us -> 13.7 us  [to_partner(): return lax.ppermute(value, 'ep_1', [(0, 1), (1, 0)])]
  transfers between devices with their start and end apart: 5 -> 2, of which waited for: 2 -> 0; matrix products, arithmetic and copies ran while one was open for 0% -> 0% of each run, Pallas kernels for 2% -> 2%
where the time goes in v3:
time: 172 us; the launch traced here: 171 us
  blocking collectives  98.6 us (57%)
  Pallas kernels  58.2 us (34%)
  starting transfers between devices  13.7 us (8%)
    all_to_all x4, blocking collectives, exchange(): return lax.all_to_all(value, axis, 0, 0, tiled=True)  98.6 us
    pallas_call x1, Pallas kernels, steps(): kernel(plan_kernel, in_specs=[hbm] * 4, out_specs=(vmem, vmem, vmem, vmem...  48.9 us
    ppermute x2, starting transfers between devices, to_partner(): return lax.ppermute(value, 'ep_1', [(0, 1), (1, 0)])  13.7 us
  transfers between devices with their start and end apart: 2, of which 0 were waited for; matrix products, arithmetic and copies ran while one was open for 0% of the time, Pallas kernels for 2%

profile of v3, /device:TPU:1, one launch (start us, length us, event | category | flops | bytes accessed | tf_op | source)
XLA Modules:
  0.0 171.2 jit_solution(11002708562581267567)
XLA Ops:
  0.6 48.9 %shard_map.111 = (bf16[592,640]{1,0:T(8,128)(2,1)S(1)}, bf16[384,296]{1,0:T(8,128)(2,1)S(1)}, bf16[384,384]{1,0:T(8,128)(2,1)S(1)}, bf16[256,128]{1,0:T(8,128)(2,1)S(1)}, bf16[6144,128]{1,0:T(8,128)(2,1)}) custom-call(s32[2,128]{1,0:T(2,128)} %bitcast.23, bf16[2048,128]{1,0:T(8,128)(2,1)} %bitcast.13, bf16[2048,128]{1,0:T(8,128)(2,1)} %bitcast.15, ...), custom_call_target="tpu_custom_call" | custom-call | tf_op jit(solution)/shard_map/pallas_call | solution.py:324
  49.6 8.7 %collective-permute-start = (bf16[6144,128]{1,0:T(8,128)(2,1)}, bf16[6144,128]{1,0:T(8,128)(2,1)S(1)}, u32[]{:S(2)}, u32[]{:S(2)}) collective-permute-start(bf16[6144,128]{1,0:T(8,128)(2,1)} %get-tuple-element.20), channel_id=1, source_target_pairs={{0,16},{16,0},{1,17},{17,1},{2,18},{18,2},{3,19},{19,3},{4,20},{20... | collective-permute-start | bytes 4718600 | tf_op jit(solution)/shard_map/ppermute | solution.py:303
  58.3 1.3 shard_map.110
  59.6 22.4 %all_to_all.20 = bf16[16,40,128]{2,1,0:T(8,128)(2,1)S(1)} all-to-all(bf16[16,40,128]{2,1,0:T(8,128)(2,1)S(1)} %bitcast.20), channel_id=1, replica_groups=mesh['ep_0'=16,'ep_1'=2,'tp'=16] {'ep_0'}, dimensions={0} | all-to-all | bytes 327680 | tf_op jit(solution)/shard_map/all_to_all | solution.py:299
  82.0 0.0 collective-permute-done.swap_ref
  82.0 0.4 shard_map.112
  82.4 0.0 copy-start
  82.5 0.0 copy-start.1
  82.5 0.0 copy-start.2
  82.5 37.1 %all_to_all.21.own_ref = bf16[16,584,128]{2,1,0:T(8,128)(2,1)S(1)} all-to-all(bf16[16,584,128]{2,1,0:T(8,128)(2,1)S(1)} %shard_map.112), channel_id=1, replica_groups=mesh['ep_0'=16,'ep_1'=2,'tp'=16] {'tp'}, dimensions={0} | all-to-all | bytes 4784128 | tf_op jit(solution)/shard_map/all_to_all | solution.py:299
  119.5 0.0 copy-done
  119.5 0.0 copy-done.1
  119.5 0.0 copy-done.2
  119.5 2.4 %shard_map.113 = (bf16[16,296,128]{2,1,0:T(8,128)(2,1)S(1)}, bf16[288,512]{1,0:T(8,128)(2,1)S(1)}, bf16[288,256]{1,0:T(8,128)(2,1)S(1)}) custom-call(bf16[16,584,128]{2,1,0:T(8,128)(2,1)S(1)} %all_to_all.21.own_ref, bf16[2048,128]{1,0:T(8,128)(2,1)S(1)} %bitcast.14, bf16[2048,128]{1,0:T(8,128)(2,1)S(1)} %bitcast.16, bf16[128,2048]{1,0:T(8,128)(2,1)S(1)} %bitcast.18, ...), custom_call_target="tpu_custom_call" | custom-call | tf_op jit(solution)/shard_map/pallas_call | solution.py:343
  122.0 1.3 shard_map.116
  123.2 4.9 %collective-permute-start.1 = (bf16[384,2048]{1,0:T(8,128)(2,1)S(1)}, bf16[384,2048]{1,0:T(8,128)(2,1)S(1)}, u32[]{:S(2)}, u32[]{:S(2)}) collective-permute-start(bf16[384,2048]{1,0:T(8,128)(2,1)S(1)} %shard_map.116), channel_id=1, source_target_pairs={{0,16},{16,0},{1,17},{17,1},{2,18},{18,2},{3,19},{19,3},{4,20},{20... | collective-permute-start | bytes 4718600 | tf_op jit(solution)/shard_map/ppermute | solution.py:303
  128.2 21.4 %all_to_all.22.in_ref = bf16[16,296,128]{2,1,0:T(8,128)(2,1)S(1)} all-to-all(bf16[16,296,128]{2,1,0:T(8,128)(2,1)S(1)} %get-tuple-element.24), channel_id=1, replica_groups=mesh['ep_0'=16,'ep_1'=2,'tp'=16] {'tp'}, dimensions={0} | all-to-all | bytes 2424832 | tf_op jit(solution)/shard_map/all_to_all | solution.py:299
  149.5 0.3 shard_map.114
  149.9 17.8 %all_to_all.23 = bf16[16,24,128]{2,1,0:T(8,128)(2,1)S(1)} all-to-all(bf16[16,24,128]{2,1,0:T(8,128)(2,1)S(1)} %bitcast.22), channel_id=1, replica_groups=mesh['ep_0'=16,'ep_1'=2,'tp'=16] {'ep_0'}, dimensions={0} | all-to-all | bytes 196608 | tf_op jit(solution)/shard_map/all_to_all | solution.py:299
  167.7 1.1 shard_map.115
  168.8 0.0 collective-permute-done.1.other_ref
  168.8 2.4 %shard_map.117 = (bf16[2048,128]{1,0:T(8,128)(2,1)}, bf16[2048,128]{1,0:T(8,128)(2,1)}, bf16[128,2048]{1,0:T(8,128)(2,1)}) custom-call(bf16[16,584,128]{2,1,0:T(8,128)(2,1)S(1)} %all_to_all.21.own_ref, bf16[288,512]{1,0:T(8,128)(2,1)S(1)} %get-tuple-element.30.both_ref, bf16[288,256]{1,0:T(8,128)(2,1)S(1)} %get-tuple-element.31.hidden_ref, ...), custom_call_target="tpu_custom_call" | custom-call | tf_op jit(solution)/shard_map/pallas_call | solution.py:352
Async XLA Ops:
  49.6 32.5 %collective-permute-start = (bf16[6144,128]{1,0:T(8,128)(2,1)}, bf16[6144,128]{1,0:T(8,128)(2,1)S(1)}, u32[]{:S(2)}, u32[]{:S(2)}) collective-permute-start(bf16[6144,128]{1,0:T(8,128)(2,1)} %get-tuple-element.20), channel_id=1, source_target_pairs={{0,16},{16,0},{1,17},{17,1},{2,18},{18,2},{3,19},{19,3},{4,20},{20... | collective-permute-start | bytes 4718600 | tf_op jit(solution)/shard_map/ppermute | solution.py:303
  82.4 37.1 %copy-start = (bf16[1,2048,128]{2,1,0:T(8,128)(2,1)S(1)}, bf16[1,2048,128]{2,1,0:T(8,128)(2,1)}, u32[]{:S(2)}) copy-start(bf16[1,2048,128]{2,1,0:T(8,128)(2,1)} %param.11) | copy-start | bytes 1572868
  82.5 37.1 %copy-start.1 = (bf16[1,2048,128]{2,1,0:T(8,128)(2,1)S(1)}, bf16[1,2048,128]{2,1,0:T(8,128)(2,1)}, u32[]{:S(2)}) copy-start(bf16[1,2048,128]{2,1,0:T(8,128)(2,1)} %param.12) | copy-start | bytes 1572868
  82.5 37.1 %copy-start.2 = (bf16[1,128,2048]{2,1,0:T(8,128)(2,1)S(1)}, bf16[1,128,2048]{2,1,0:T(8,128)(2,1)}, u32[]{:S(2)}) copy-start(bf16[1,128,2048]{2,1,0:T(8,128)(2,1)} %param.13) | copy-start | bytes 1572868
  123.2 45.6 %collective-permute-start.1 = (bf16[384,2048]{1,0:T(8,128)(2,1)S(1)}, bf16[384,2048]{1,0:T(8,128)(2,1)S(1)}, u32[]{:S(2)}, u32[]{:S(2)}) collective-permute-start(bf16[384,2048]{1,0:T(8,128)(2,1)S(1)} %shard_map.116), channel_id=1, source_target_pairs={{0,16},{16,0},{1,17},{17,1},{2,18},{18,2},{3,19},{19,3},{4,20},{20... | collective-permute-start | bytes 4718600 | tf_op jit(solution)/shard_map/ppermute | solution.py:303

commit v4 on v3

--- a/solution.py
+++ b/solution.py
@@ -96,11 +96,7 @@
     out_ref[...] = rows.reshape(16 * PIECE, 128).astype(BF)
 
 
-def plan_kernel(
-    routes_hbm, gate, up, down, copies_ref, back_ref, combine_ref, lanes_ref, swap_ref, routes_ref, sems
-):
-    routes_load = pltpu.make_async_copy(routes_hbm, routes_ref, sems.at[18])
-    routes_load.start()
+def plan_kernel(gate, up, down, copies_ref, swap_ref, sems):
     moves = [
         pltpu.make_async_copy(ref, swap_ref.at[pl.ds(2048 * k, 2048), :], sems.at[16 + k])
         for k, ref in enumerate((gate, up))
@@ -125,14 +121,13 @@
     pick = ((of_source >> 2) == (i & 3)) & (within == jnp.where(i >= 4, 37, 36)) & (i < 8)
     copies_ref[2 * ROWS : 2 * ROWS + 16, :] = one_if(pick)
 
-    p = iota((SRC * BACK, 1), 0)
-    source = (p * 2731) >> 16
-    j = p - source * BACK
-    target = jnp.where(j < CAP, source * CAP + j, -1)
-    target = jnp.where(j == 18, ROWS + (source >> 2), target)
-    target = jnp.where(j == 19, ROWS + 4 + (source >> 2), target)
-    back_ref[...] = one_if(iota((SRC * BACK, PART), 1) == target)
-
+    for move in moves:
+        move.wait()
+
+
+def places_kernel(routes_hbm, combine_ref, lanes_ref, routes_ref, sem):
+    routes_load = pltpu.make_async_copy(routes_hbm, routes_ref, sem)
+    routes_load.start()
     routes_load.wait()
     routes = routes_ref[...]
     first, second, member, rank = ranks(routes)
@@ -151,8 +146,6 @@
         index = jnp.sum(jnp.where(mine, rank, 0.0), axis=0, keepdims=True).astype(jnp.int32)
         lanes = jnp.where(iota((128, 128), 0) == index + offset, 1.0, 0.0)
         lanes_ref[128 * k : 128 * (k + 1), :] = jnp.transpose(lanes).astype(BF)
-    for move in moves:
-        move.wait()
 
 
 def copies_kernel(in_ref, pick_ref, out_ref):
@@ -247,14 +240,21 @@
         down_out[:, cols] = (down + other_ref[256:384, cols].astype(F32)).astype(BF)
 
 
-def sum_kernel(in_ref, pick_ref, out_ref):
+def sum_kernel(in_ref, out_ref):
     rows = in_ref[0].astype(F32)
     for t in range(1, 16):
         rows = rows + in_ref[t].astype(F32)
     packed = rows[ROWS : ROWS + 4] + rows[ROWS + 4 : PART]
     high = packed.astype(BF).astype(F32)
     rows = jnp.concatenate([rows[:ROWS], high, packed - high], axis=0).astype(BF)
-    out_ref[...] = matmul(pick_ref[...], rows).astype(BF)
+    p = iota((SRC * BACK, 1), 0)
+    source = (p * 2731) >> 16
+    j = p - source * BACK
+    target = jnp.where(j < CAP, source * CAP + j, -1)
+    target = jnp.where(j == 18, ROWS + (source >> 2), target)
+    target = jnp.where(j == 19, ROWS + 4 + (source >> 2), target)
+    pick = one_if(iota((SRC * BACK, PART), 1) == target)
+    out_ref[...] = matmul(pick, rows).astype(BF)
 
 
 def combine_kernel(in_ref, pick_ref, lanes_ref, tokens_ref, route_ref):
@@ -273,10 +273,6 @@
 
 def shape(dims, dtype=BF):
     return jax.ShapeDtypeStruct(dims, dtype)
-
-
-def far_shape(dims, dtype=BF):
-    return pltpu.HBM(dims, dtype)
 
 
 def near(dims, dtype=BF):
@@ -321,19 +317,13 @@
         scratch_shapes=[pltpu.VMEM((256, 128), BF), *small, pltpu.SemaphoreType.DMA((4,))],
     )(far(routes_t), far(weights_t), far(tokens), far(out_grad))
     received = exchange(pieces.reshape(16, PIECE, 128), "ep_0")
-    pick_copies, pick_back, pick_combine, lanes, packed = kernel(
+    pick_copies, packed = kernel(
         plan_kernel,
-        in_specs=[hbm] * 4,
-        out_specs=(vmem, vmem, vmem, vmem, hbm),
-        out_shape=(
-            near((2 * ROWS + 16, SRC * PIECE)),
-            shape((SRC * BACK, PART)),
-            shape((384, 16 * BACK)),
-            shape((256, 128)),
-            far_shape((3 * width, 128)),
-        ),
-        scratch_shapes=[small[0], pltpu.SemaphoreType.DMA((19,))],
-    )(far(routes_t), far(gate), far(up), far(down))
+        in_specs=[hbm] * 3,
+        out_specs=(vmem, vmem),
+        out_shape=(near((2 * ROWS + 16, SRC * PIECE)), near((3 * width, 128))),
+        scratch_shapes=[pltpu.SemaphoreType.DMA((18,))],
+    )(far(gate), far(up), far(down))
     packed_2 = to_partner(packed)
     received, packed_2 = lax.optimization_barrier((received, packed_2))
     copies = kernel(copies_kernel, out_shape=near((16, GATH, 128)))(
@@ -352,7 +342,14 @@
     gate_grad, up_grad, down_grad = kernel(
         own_grads_kernel, out_shape=(shape((width, 128)), shape((width, 128)), shape((128, width)))
     )(own, both, hidden, mine)
-    back = kernel(sum_kernel, out_shape=near((SRC * BACK, 128)))(hold(spread), hold(pick_back))
+    back = kernel(sum_kernel, out_shape=near((SRC * BACK, 128)))(hold(spread))
+    pick_combine, lanes = kernel(
+        places_kernel,
+        in_specs=[hbm],
+        out_specs=(vmem, vmem),
+        out_shape=(near((384, 16 * BACK)), near((256, 128))),
+        scratch_shapes=[small[0], pltpu.SemaphoreType.DMA],
+    )(far(routes_t))
     home = exchange(back.reshape(SRC, BACK, 128), "ep_0")
     tokens_grad, route_grad = kernel(
         combine_kernel, out_shape=(shape((count, 128)), shape((2, count), F32))

time: 172 us -> 128 us (0.74)
  Pallas kernels: 58.2 us -> 15 us
  blocking collectives: 98.6 us -> 80.8 us
  waiting for transfers between devices: 0.01 us -> 10.9 us
  starting transfers between devices: 13.7 us -> 19.8 us
    pallas_call x2 -> x3, Pallas kernels: 49.3 us -> 3.46 us  [the longest x1 1.43 us: steps(): kernel(plan_kernel, in_specs=[hbm] * 3, out_specs=(vmem, vmem), out_shape...]
    all_to_all x4 -> x3, blocking collectives: 98.6 us -> 80.8 us  [exchange(): return lax.all_to_all(value, axis, 0, 0, tiled=True)]
    all_to_all x0 -> x1, waiting for transfers between devices: none -> 10.9 us  [exchange(): return lax.all_to_all(value, axis, 0, 0, tiled=True)]
    all_to_all x0 -> x1, starting transfers between devices: none -> 6.16 us  [exchange(): return lax.all_to_all(value, axis, 0, 0, tiled=True)]
  transfers between devices with their start and end apart: 2 -> 3, of which waited for: 0 -> 1; matrix products, arithmetic and copies ran while one was open for 0% -> 0% of each run, Pallas kernels for 2% -> 4%
where the time goes in v4:
time: 128 us; the launch traced here: 127 us
  blocking collectives  80.8 us (63%)
  starting transfers between devices  19.8 us (15%)
  Pallas kernels  15 us (12%)
  waiting for transfers between devices  10.9 us (9%)
    all_to_all x3, blocking collectives, exchange(): return lax.all_to_all(value, axis, 0, 0, tiled=True)  80.8 us
    ppermute x2, starting transfers between devices, to_partner(): return lax.ppermute(value, 'ep_1', [(0, 1), (1, 0)])  13.7 us
    all_to_all x1, waiting for transfers between devices, exchange(): return lax.all_to_all(value, axis, 0, 0, tiled=True)  10.9 us
    all_to_all x1, starting transfers between devices, exchange(): return lax.all_to_all(value, axis, 0, 0, tiled=True)  6.16 us
    pallas_call x1, Pallas kernels, steps(): kernel(own_grads_kernel, out_shape=(shape((width, 128)), shape((width, 12...  3.8 us
  transfers between devices with their start and end apart: 3, of which 1 were waited for; matrix products, arithmetic and copies ran while one was open for 0% of the time, Pallas kernels for 4%

profile of v4, /device:TPU:1, one launch (start us, length us, event | category | flops | bytes accessed | tf_op | source)
XLA Modules:
  0.0 127.2 jit_solution(1632791404306565006)
XLA Ops:
  0.6 1.4 %shard_map.111 = (bf16[592,640]{1,0:T(8,128)(2,1)S(1)}, bf16[6144,128]{1,0:T(8,128)(2,1)S(1)}) custom-call(bf16[2048,128]{1,0:T(8,128)(2,1)} %bitcast.13, bf16[2048,128]{1,0:T(8,128)(2,1)} %bitcast.15, bf16[128,2048]{1,0:T(8,128)(2,1)} %bitcast.17), custom_call_target="tpu_custom_call" | custom-call | tf_op jit(solution)/shard_map/pallas_call | solution.py:320
  2.1 8.7 %collective-permute-start = (bf16[6144,128]{1,0:T(8,128)(2,1)S(1)}, bf16[6144,128]{1,0:T(8,128)(2,1)S(1)}, u32[]{:S(2)}, u32[]{:S(2)}) collective-permute-start(bf16[6144,128]{1,0:T(8,128)(2,1)S(1)} %get-tuple-element.19), channel_id=1, source_target_pairs={{0,16},{16,0},{1,17},{17,1},{2,18},{18,2},{3,19},{19,3},{4,20},{20... | collective-permute-start | bytes 4718600 | tf_op jit(solution)/shard_map/ppermute | solution.py:299
  10.8 1.3 %shard_map.110 = bf16[640,128]{1,0:T(8,128)(2,1)S(1)} custom-call(s32[2,128]{1,0:T(2,128)} %bitcast.23, f32[2,128]{1,0:T(2,128)} %bitcast.22, bf16[128,2048]{1,0:T(8,128)(2,1)} %tokens_ref.1, bf16[128,2048]{1,0:T(8,128)(2,1)} %grad_ref.1), custom_call_target="tpu_custom_call" | custom-call | tf_op jit(solution)/shard_map/pallas_call | solution.py:313
  12.1 22.4 %all_to_all.20 = bf16[16,40,128]{2,1,0:T(8,128)(2,1)S(1)} all-to-all(bf16[16,40,128]{2,1,0:T(8,128)(2,1)S(1)} %bitcast.20), channel_id=1, replica_groups=mesh['ep_0'=16,'ep_1'=2,'tp'=16] {'ep_0'}, dimensions={0} | all-to-all | bytes 327680 | tf_op jit(solution)/shard_map/all_to_all | solution.py:295
  34.5 0.0 collective-permute-done.swap_ref
  34.5 0.4 shard_map.112
  34.9 0.0 copy-start
  35.0 0.0 copy-start.1
  35.0 0.0 copy-start.2
  35.0 37.1 %all_to_all.21.own_ref = bf16[16,584,128]{2,1,0:T(8,128)(2,1)S(1)} all-to-all(bf16[16,584,128]{2,1,0:T(8,128)(2,1)S(1)} %shard_map.112), channel_id=1, replica_groups=mesh['ep_0'=16,'ep_1'=2,'tp'=16] {'tp'}, dimensions={0} | all-to-all | bytes 4784128 | tf_op jit(solution)/shard_map/all_to_all | solution.py:295
  72.0 0.0 copy-done
  72.0 0.0 copy-done.1
  72.0 0.0 copy-done.2
  72.0 2.4 %shard_map.113 = (bf16[16,296,128]{2,1,0:T(8,128)(2,1)S(1)}, bf16[288,512]{1,0:T(8,128)(2,1)S(1)}, bf16[288,256]{1,0:T(8,128)(2,1)S(1)}) custom-call(bf16[16,584,128]{2,1,0:T(8,128)(2,1)S(1)} %all_to_all.21.own_ref, bf16[2048,128]{1,0:T(8,128)(2,1)S(1)} %bitcast.14, bf16[2048,128]{1,0:T(8,128)(2,1)S(1)} %bitcast.16, bf16[128,2048]{1,0:T(8,128)(2,1)S(1)} %bitcast.18, ...), custom_call_target="tpu_custom_call" | custom-call | tf_op jit(solution)/shard_map/pallas_call | solution.py:333
  74.5 2.4 %shard_map.117 = bf16[384,2048]{1,0:T(8,128)(2,1)} custom-call(bf16[16,584,128]{2,1,0:T(8,128)(2,1)S(1)} %all_to_all.21.own_ref, bf16[288,512]{1,0:T(8,128)(2,1)S(1)} %get-tuple-element.28.both_ref, bf16[288,256]{1,0:T(8,128)(2,1)S(1)} %get-tuple-element.29.hidden_ref), custom_call_target="tpu_custom_call" | custom-call | tf_op jit(solution)/shard_map/pallas_call | solution.py:340
  76.9 4.9 %collective-permute-start.1 = (bf16[384,2048]{1,0:T(8,128)(2,1)}, bf16[384,2048]{1,0:T(8,128)(2,1)}, u32[]{:S(2)}, u32[]{:S(2)}) collective-permute-start(bf16[384,2048]{1,0:T(8,128)(2,1)} %shard_map.117), channel_id=1, source_target_pairs={{0,16},{16,0},{1,17},{17,1},{2,18},{18,2},{3,19},{19,3},{4,20},{20... | collective-permute-start | bytes 4718600 | tf_op jit(solution)/shard_map/ppermute | solution.py:299
  81.8 21.4 %all_to_all.22.in_ref = bf16[16,296,128]{2,1,0:T(8,128)(2,1)S(1)} all-to-all(bf16[16,296,128]{2,1,0:T(8,128)(2,1)S(1)} %get-tuple-element.23), channel_id=1, replica_groups=mesh['ep_0'=16,'ep_1'=2,'tp'=16] {'tp'}, dimensions={0} | all-to-all | bytes 2424832 | tf_op jit(solution)/shard_map/all_to_all | solution.py:295
  103.2 1.1 shard_map.114
  104.3 6.2 %all-to-all-start.3 = ((bf16[16,24,128]{2,1,0:T(8,128)(2,1)}), bf16[16,24,128]{2,1,0:T(8,128)(2,1)S(1)}, u32[]{:S(2)}, u32[]{:S(2)}) async-start(bf16[16,24,128]{2,1,0:T(8,128)(2,1)} %bitcast.7), calls=%async_computation.3 | async-start | bytes 196608 | tf_op jit(solution)/shard_map/all_to_all | solution.py:295
  110.4 1.0 shard_map.115
  111.4 10.9 %all-to-all-done.3 = bf16[16,24,128]{2,1,0:T(8,128)(2,1)S(1)} async-done(((bf16[16,24,128]{2,1,0:T(8,128)(2,1)}), bf16[16,24,128]{2,1,0:T(8,128)(2,1)S(1)}, u32[]{:S(2)}, u32[]{:S(2)}) %all-to-all-start.3) | async-done | bytes 98336 | tf_op jit(solution)/shard_map/all_to_all | solution.py:295
  122.3 1.1 shard_map.116
  123.4 0.0 collective-permute-done.1.other_ref
  123.4 3.8 %shard_map.118 = (bf16[2048,128]{1,0:T(8,128)(2,1)}, bf16[2048,128]{1,0:T(8,128)(2,1)}, bf16[128,2048]{1,0:T(8,128)(2,1)}) custom-call(bf16[16,584,128]{2,1,0:T(8,128)(2,1)S(1)} %all_to_all.21.own_ref, bf16[288,512]{1,0:T(8,128)(2,1)S(1)} %get-tuple-element.28.both_ref, bf16[288,256]{1,0:T(8,128)(2,1)S(1)} %get-tuple-element.29.hidden_ref, ...), custom_call_target="tpu_custom_call" | custom-call | tf_op jit(solution)/shard_map/pallas_call | solution.py:342
Async XLA Ops:
  2.1 32.5 %collective-permute-start = (bf16[6144,128]{1,0:T(8,128)(2,1)S(1)}, bf16[6144,128]{1,0:T(8,128)(2,1)S(1)}, u32[]{:S(2)}, u32[]{:S(2)}) collective-permute-start(bf16[6144,128]{1,0:T(8,128)(2,1)S(1)} %get-tuple-element.19), channel_id=1, source_target_pairs={{0,16},{16,0},{1,17},{17,1},{2,18},{18,2},{3,19},{19,3},{4,20},{20... | collective-permute-start | bytes 4718600 | tf_op jit(solution)/shard_map/ppermute | solution.py:299
  34.9 37.1 %copy-start = (bf16[1,2048,128]{2,1,0:T(8,128)(2,1)S(1)}, bf16[1,2048,128]{2,1,0:T(8,128)(2,1)}, u32[]{:S(2)}) copy-start(bf16[1,2048,128]{2,1,0:T(8,128)(2,1)} %param.11) | copy-start | bytes 1572868
  35.0 37.1 %copy-start.1 = (bf16[1,2048,128]{2,1,0:T(8,128)(2,1)S(1)}, bf16[1,2048,128]{2,1,0:T(8,128)(2,1)}, u32[]{:S(2)}) copy-start(bf16[1,2048,128]{2,1,0:T(8,128)(2,1)} %param.12) | copy-start | bytes 1572868
  35.0 37.1 %copy-start.2 = (bf16[1,128,2048]{2,1,0:T(8,128)(2,1)S(1)}, bf16[1,128,2048]{2,1,0:T(8,128)(2,1)}, u32[]{:S(2)}) copy-start(bf16[1,128,2048]{2,1,0:T(8,128)(2,1)} %param.13) | copy-start | bytes 1572868
  76.9 46.5 %collective-permute-start.1 = (bf16[384,2048]{1,0:T(8,128)(2,1)}, bf16[384,2048]{1,0:T(8,128)(2,1)}, u32[]{:S(2)}, u32[]{:S(2)}) collective-permute-start(bf16[384,2048]{1,0:T(8,128)(2,1)} %shard_map.117), channel_id=1, source_target_pairs={{0,16},{16,0},{1,17},{17,1},{2,18},{18,2},{3,19},{19,3},{4,20},{20... | collective-permute-start | bytes 4718600 | tf_op jit(solution)/shard_map/ppermute | solution.py:299
  104.3 18.0 %all-to-all-start.3 = ((bf16[16,24,128]{2,1,0:T(8,128)(2,1)}), bf16[16,24,128]{2,1,0:T(8,128)(2,1)S(1)}, u32[]{:S(2)}, u32[]{:S(2)}) async-start(bf16[16,24,128]{2,1,0:T(8,128)(2,1)} %bitcast.7), calls=%async_computation.3 | async-start | bytes 196608 | tf_op jit(solution)/shard_map/all_to_all | solution.py:295

commit v5 on v4

--- a/solution.py
+++ b/solution.py
@@ -14,11 +14,11 @@
 CAP = 18
 SRC = 16
 ROWS = SRC * CAP
-PIECE = 40
-BACK = 24
-GATH = 2 * ROWS + 8
+PIECE = 36
+BACK = 20
+GATH = 2 * ROWS
+PART = ROWS + 8
 LIMIT = pltpu.CompilerParams(vmem_limit_bytes=24 * 1024 * 1024)
-PART = ROWS + 8
 
 
 def iota(shape, dim):
@@ -41,6 +41,10 @@
 
 def matmul(left, right):
     return lax.dot_general(left, right, (((1,), (0,)), ((), ())), preferred_element_type=F32)
+
+
+def expand(expert, values):
+    return matmul(one_if(iota((expert.shape[0], 16), 1) == expert), values)
 
 
 def ranks(routes):
@@ -75,25 +79,22 @@
     first, second, member, rank = ranks(routes_ref[...])
     weights = weights_ref[...]
     weight = jnp.where(first, weights[0:1, :], 0.0) + jnp.where(second, weights[1:2, :], 0.0)
-    slot = jnp.where(member > 0.0, rank, -100.0).astype(jnp.int32)
-    row = iota((16, PIECE, 128), 1)
-    slot_3 = jnp.broadcast_to(slot[:, None, :], (16, PIECE, 128))
-    sel_x = jnp.where(slot_3 == row, 1.0, 0.0)
-    sel_dy = jnp.where(slot_3 + CAP == row, 1.0, 0.0)
-    chosen = jnp.concatenate(
-        [sel_x.reshape(16 * PIECE, 128).astype(BF), sel_dy.reshape(16 * PIECE, 128).astype(BF)], axis=1
-    )
-    value = jnp.sum(sel_x * weight[:, None, :], axis=2, keepdims=True)
-    offset = (lax.axis_index("ep_0") % 4) * 32
-    spread = jnp.where(iota((16, PIECE, 128), 2) == row + offset, value, 0.0)
-    packed = jnp.sum(jnp.where(row < CAP, spread, 0.0), axis=1, keepdims=True)
-    high = packed.astype(BF).astype(F32)
-    low = packed - high
+    slot = jnp.where(member > 0.0, rank, -100.0)
+    row = iota((16 * PIECE, 1), 0)
+    expert = (row * 1821) >> 16
+    slots = expand(expert, slot.astype(BF)).astype(jnp.int32)
+    within = row - expert * PIECE
+    sel_x = slots == within
+    sel_dy = slots + CAP == within
+    high, low = split_two(weight)
+    lowest = (weight - high.astype(F32) - low.astype(F32)).astype(BF)
+    spread = expand(expert, high) + expand(expert, low) + expand(expert, lowest)
+    factor = jnp.sum(jnp.where(sel_dy, spread, 0.0), axis=1, keepdims=True)
+    factor = jnp.where(within < CAP, 1.0, factor)
+    chosen = jnp.concatenate([one_if(sel_x), one_if(sel_dy)], axis=1)
     for load in loads:
         load.wait()
-    rows = matmul(chosen, data_ref[...]).reshape(16, PIECE, 128)
-    rows = jnp.where(row == 36, high, jnp.where(row == 37, low, rows))
-    out_ref[...] = rows.reshape(16 * PIECE, 128).astype(BF)
+    out_ref[...] = (matmul(chosen, data_ref[...]) * factor).astype(BF)
 
 
 def plan_kernel(gate, up, down, copies_ref, swap_ref, sems):
@@ -108,50 +109,51 @@
     ]
     for move in moves:
         move.start()
-    p = iota((2 * ROWS, 1), 0)
+    p = iota((GATH, 1), 0)
     is_dy = p >= ROWS
     q = jnp.where(is_dy, p - ROWS, p)
     source = (q * 3641) >> 16
     target = source * PIECE + (q - source * CAP) + jnp.where(is_dy, CAP, 0)
-    copies_ref[0 : 2 * ROWS, :] = one_if(iota((2 * ROWS, SRC * PIECE), 1) == target)
-    col = iota((16, SRC * PIECE), 1)
-    of_source = (col * 1639) >> 16
-    within = col - of_source * PIECE
-    i = iota((16, SRC * PIECE), 0)
-    pick = ((of_source >> 2) == (i & 3)) & (within == jnp.where(i >= 4, 37, 36)) & (i < 8)
-    copies_ref[2 * ROWS : 2 * ROWS + 16, :] = one_if(pick)
-
+    copies_ref[...] = one_if(iota((GATH, SRC * PIECE), 1) == target)
     for move in moves:
         move.wait()
 
 
-def places_kernel(routes_hbm, combine_ref, lanes_ref, routes_ref, sem):
-    routes_load = pltpu.make_async_copy(routes_hbm, routes_ref, sem)
-    routes_load.start()
-    routes_load.wait()
+def places_kernel(routes_hbm, weights_hbm, combine_ref, lanes_ref, routes_ref, weights_ref, sems):
+    loads = [
+        pltpu.make_async_copy(routes_hbm, routes_ref, sems.at[0]),
+        pltpu.make_async_copy(weights_hbm, weights_ref, sems.at[1]),
+    ]
+    for load in loads:
+        load.start()
+    for load in loads:
+        load.wait()
     routes = routes_ref[...]
     first, second, member, rank = ranks(routes)
-    slot = jnp.where(member > 0.0, rank, -100.0).astype(jnp.int32)
-    row = iota((16, BACK, 128), 1)
-    sel = jnp.where(jnp.broadcast_to(slot[:, None, :], (16, BACK, 128)) == row, 1.0, 0.0)
-    combine_ref[0:128, :] = jnp.transpose(sel.reshape(16 * BACK, 128)).astype(BF)
+    slot = jnp.where(member > 0.0, rank, -100.0)
+    row = iota((16 * BACK, 1), 0)
+    expert = (row * 3277) >> 16
+    within = row - expert * BACK
+    sel = jnp.where(expand(expert, slot.astype(BF)).astype(jnp.int32) == within, 1.0, 0.0)
+    combine_ref[0:128, :] = jnp.transpose(sel).astype(BF)
     offset = (lax.axis_index("ep_0") % 4) * 32
-    is_gate = (row == 18) | (row == 19)
+    weights = weights_ref[...]
     for k, mine in enumerate((first, second)):
-        chosen = jnp.where(mine, 1.0, 0.0)[:, None, :]
-        sel = jnp.where(is_gate, jnp.broadcast_to(chosen, (16, BACK, 128)), 0.0)
-        combine_ref[128 * (k + 1) : 128 * (k + 2), :] = jnp.transpose(
-            sel.reshape(16 * BACK, 128)
-        ).astype(BF)
+        sel = jnp.where(within >= CAP, expand(expert, one_if(mine)), 0.0)
+        combine_ref[128 * (k + 1) : 128 * (k + 2), :] = jnp.transpose(sel).astype(BF)
         index = jnp.sum(jnp.where(mine, rank, 0.0), axis=0, keepdims=True).astype(jnp.int32)
-        lanes = jnp.where(iota((128, 128), 0) == index + offset, 1.0, 0.0)
-        lanes_ref[128 * k : 128 * (k + 1), :] = jnp.transpose(lanes).astype(BF)
+        lanes = jnp.where(iota((128, 128), 0) == index + offset, 1.0 / weights[k : k + 1, :], 0.0)
+        lanes_ref[128 * k : 128 * (k + 1), :] = jnp.transpose(lanes)
+
+
+def settle_kernel(in_ref, out_ref):
+    del in_ref, out_ref
 
 
 def copies_kernel(in_ref, pick_ref, out_ref):
     rows = matmul(pick_ref[...], in_ref[...]).astype(BF)
     for t in range(16):
-        out_ref[t] = rows[:GATH]
+        out_ref[t] = rows
 
 
 def lane_of_row():
@@ -159,12 +161,6 @@
     source = (r * 3641) >> 16
     lane = (source & 3) * 32 + (r - source * CAP)
     return source >> 2, lane
-
-
-def row_weights(extra):
-    group, lane = lane_of_row()
-    spread = matmul(one_if((iota((ROWS, 8), 1) & 3) == group), extra)
-    return jnp.sum(jnp.where(iota((ROWS, 128), 1) == lane, spread, 0.0), axis=1, keepdims=True)
 
 
 def pair_cols(ref, t, start):
@@ -194,9 +190,8 @@
     activ = pre_gate * sigma
     hidden = activ * pre_up
     gate_part = jnp.sum(hidden * d_hidden, axis=1, keepdims=True)
-    scaled = row_weights(own_ref[0, 2 * ROWS : GATH, :]) * d_hidden
-    d_gate = (scaled * pre_up * sigma * (1.0 + pre_gate * (1.0 - sigma))).astype(BF)
-    d_up = (scaled * activ).astype(BF)
+    d_gate = (d_hidden * pre_up * sigma * (1.0 + pre_gate * (1.0 - sigma))).astype(BF)
+    d_up = (d_hidden * activ).astype(BF)
     both_ref[:, 0:256] = d_gate
     both_ref[:, 256:512] = d_up
     hidden_ref[...] = hidden.astype(BF)
@@ -219,11 +214,10 @@
     both = jnp.concatenate([both_ref[:, lanes], both_ref[:, late]], axis=1)
     both_t = jnp.transpose(both.astype(F32)).astype(BF)
     hidden_t = jnp.transpose(hidden_ref[:, lanes].astype(F32)).astype(BF)
-    g = row_weights(own_ref[0, 2 * ROWS : GATH, :])
     for t in range(8):
         cols = slice(256 * t, 256 * t + 256)
-        scaled = (g * pair_cols(own_ref, t, ROWS).astype(F32)).astype(BF)
-        yield cols, matmul(both_t, pair_cols(own_ref, t, 0)), matmul(hidden_t, scaled)
+        grads = matmul(both_t, pair_cols(own_ref, t, 0))
+        yield cols, grads, matmul(hidden_t, pair_cols(own_ref, t, ROWS))
 
 
 def partner_grads_kernel(own_ref, both_ref, hidden_ref, out_ref):
@@ -248,7 +242,7 @@
     high = packed.astype(BF).astype(F32)
     rows = jnp.concatenate([rows[:ROWS], high, packed - high], axis=0).astype(BF)
     p = iota((SRC * BACK, 1), 0)
-    source = (p * 2731) >> 16
+    source = (p * 3277) >> 16
     j = p - source * BACK
     target = jnp.where(j < CAP, source * CAP + j, -1)
     target = jnp.where(j == 18, ROWS + (source >> 2), target)
@@ -262,7 +256,7 @@
     tokens_ref[...] = values[:128].astype(BF)
     gates = lax.dot_general(
         jnp.ones((8, 128), F32),
-        values[128:] * lanes_ref[...].astype(F32),
+        values[128:] * lanes_ref[...],
         (((1,), (1,)), ((), ())),
         precision=lax.Precision.HIGHEST,
         preferred_element_type=F32,
@@ -273,6 +267,10 @@
 
 def shape(dims, dtype=BF):
     return jax.ShapeDtypeStruct(dims, dtype)
+
+
+def far_shape(dims, dtype=BF):
+    return pltpu.HBM(dims, dtype)
 
 
 def near(dims, dtype=BF):
@@ -316,16 +314,22 @@
         out_shape=near((16 * PIECE, 128)),
         scratch_shapes=[pltpu.VMEM((256, 128), BF), *small, pltpu.SemaphoreType.DMA((4,))],
     )(far(routes_t), far(weights_t), far(tokens), far(out_grad))
-    received = exchange(pieces.reshape(16, PIECE, 128), "ep_0")
+    received = exchange(pieces.reshape(16, PIECE // 4, 4, 128), "ep_0")
     pick_copies, packed = kernel(
         plan_kernel,
         in_specs=[hbm] * 3,
         out_specs=(vmem, vmem),
-        out_shape=(near((2 * ROWS + 16, SRC * PIECE)), near((3 * width, 128))),
+        out_shape=(near((GATH, SRC * PIECE)), near((3 * width, 128))),
         scratch_shapes=[pltpu.SemaphoreType.DMA((18,))],
     )(far(gate), far(up), far(down))
     packed_2 = to_partner(packed)
-    received, packed_2 = lax.optimization_barrier((received, packed_2))
+    packed_2 = kernel(
+        settle_kernel,
+        in_specs=[hbm],
+        out_specs=hbm,
+        out_shape=far_shape((3 * width, 128)),
+        input_output_aliases={0: 0},
+    )(far(packed_2))
     copies = kernel(copies_kernel, out_shape=near((16, GATH, 128)))(
         hold(received.reshape(SRC * PIECE, 128)), hold(pick_copies)
     )
@@ -335,7 +339,7 @@
         in_specs=[vmem] * 5,
         out_specs=(vmem, vmem, vmem),
         out_shape=(near((16, PART, 128)), near((ROWS, 512)), near((ROWS, 256))),
-    )(own, gate, up, down, hold(packed_2))
+    )(own, gate, up, down, packed_2)
     spread = exchange(part, "tp")
     partner = kernel(partner_grads_kernel, out_shape=shape((384, width)))(own, both, hidden)
     mine = to_partner(partner)
@@ -345,12 +349,12 @@
     back = kernel(sum_kernel, out_shape=near((SRC * BACK, 128)))(hold(spread))
     pick_combine, lanes = kernel(
         places_kernel,
-        in_specs=[hbm],
+        in_specs=[hbm] * 2,
         out_specs=(vmem, vmem),
-        out_shape=(near((384, 16 * BACK)), near((256, 128))),
-        scratch_shapes=[small[0], pltpu.SemaphoreType.DMA],
-    )(far(routes_t))
-    home = exchange(back.reshape(SRC, BACK, 128), "ep_0")
+        out_shape=(near((384, 16 * BACK)), near((256, 128), F32)),
+        scratch_shapes=[*small, pltpu.SemaphoreType.DMA((2,))],
+    )(far(routes_t), far(weights_t))
+    home = exchange(back.reshape(SRC, BACK // 4, 4, 128), "ep_0")
     tokens_grad, route_grad = kernel(
         combine_kernel, out_shape=(shape((count, 128)), shape((2, count), F32))
     )(hold(home.reshape(16 * BACK, 128)), hold(pick_combine), hold(lanes))

time: 128 us -> 132 us (1.031)
  blocking collectives: 80.8 us -> 21.4 us
  waiting for transfers between devices: 10.9 us -> 40.2 us
  starting transfers between devices: 19.8 us -> 46.7 us
  local copies, waits for them, and re-layouts: 0.02 us -> 6.16 us
    all_to_all x3 -> x1, blocking collectives: 80.8 us -> 21.4 us  [exchange(): return lax.all_to_all(value, axis, 0, 0, tiled=True)]
    all_to_all x1 -> x3, waiting for transfers between devices: 10.9 us -> 37 us  [exchange(): return lax.all_to_all(value, axis, 0, 0, tiled=True)]
    all_to_all x1 -> x3, starting transfers between devices: 6.16 us -> 31.5 us  [exchange(): return lax.all_to_all(value, axis, 0, 0, tiled=True)]
    unnamed x6 -> x18, local copies, waits for them, and re-layouts: 0.02 us -> 6.16 us
    ppermute x2, waiting for transfers between devices: 0.01 us -> 3.23 us  [to_partner(): return lax.ppermute(value, 'ep_1', [(0, 1), (1, 0)])]
    ppermute x2, starting transfers between devices: 13.7 us -> 15.2 us  [to_partner(): return lax.ppermute(value, 'ep_1', [(0, 1), (1, 0)])]
  transfers between devices with their start and end apart: 3 -> 5, of which waited for: 1 -> 4; matrix products, arithmetic and copies ran while one was open for 0% -> 0% of each run, Pallas kernels for 4% -> 4%
where the time goes in v5:
time: 132 us; the launch traced here: 131 us
  starting transfers between devices  46.7 us (35%)
  waiting for transfers between devices  40.2 us (30%)
  blocking collectives  21.4 us (16%)
  Pallas kernels  15.6 us (12%)
  local copies, waits for them, and re-layouts  6.16 us (5%)
    all_to_all x3, waiting for transfers between devices, exchange(): return lax.all_to_all(value, axis, 0, 0, tiled=True)  37 us
    all_to_all x3, starting transfers between devices, exchange(): return lax.all_to_all(value, axis, 0, 0, tiled=True)  31.5 us
    all_to_all x1, blocking collectives, exchange(): return lax.all_to_all(value, axis, 0, 0, tiled=True)  21.4 us
    ppermute x2, starting transfers between devices, to_partner(): return lax.ppermute(value, 'ep_1', [(0, 1), (1, 0)])  15.2 us
    unnamed x18, local copies, waits for them, and re-layouts  6.16 us
    pallas_call x1, Pallas kernels, steps(): kernel(own_grads_kernel, out_shape=(shape((width, 128)), shape((width, 12...  3.61 us
    ppermute x2, waiting for transfers between devices, to_partner(): return lax.ppermute(value, 'ep_1', [(0, 1), (1, 0)])  3.23 us
  transfers between devices with their start and end apart: 5, of which 4 were waited for; matrix products, arithmetic and copies ran while one was open for 0% of the time, Pallas kernels for 4%

profile of v5, /device:TPU:1, one launch (start us, length us, event | category | flops | bytes accessed | tf_op | source)
XLA Modules:
  0.0 130.8 jit_solution(12762037730702022244)
XLA Ops:
  0.6 2.2 %shard_map.110 = bf16[576,128]{1,0:T(8,128)(2,1)} custom-call(s32[2,128]{1,0:T(2,128)} %bitcast.21, f32[2,128]{1,0:T(2,128)} %bitcast.23, bf16[128,2048]{1,0:T(8,128)(2,1)} %tokens_ref.1, bf16[128,2048]{1,0:T(8,128)(2,1)} %grad_ref.1), custom_call_target="tpu_custom_call" | custom-call | tf_op jit(solution)/shard_map/pallas_call | solution.py:311
  2.8 15.7 %all-to-all-start = ((bf16[16,9,4,128]{3,2,1,0:T(4,128)(2,1)}), bf16[16,9,4,128]{3,2,1,0:T(4,128)(2,1)S(1)}, u32[]{:S(2)}, u32[]{:S(2)}) async-start(bf16[16,9,4,128]{3,2,1,0:T(4,128)(2,1)} %bitcast.2), calls=%async_computation | async-start | bytes 294912 | tf_op jit(solution)/shard_map/all_to_all | solution.py:293
  18.5 1.4 %shard_map.111 = (bf16[576,576]{1,0:T(8,128)(2,1)S(1)}, bf16[6144,128]{1,0:T(8,128)(2,1)S(1)}) custom-call(bf16[2048,128]{1,0:T(8,128)(2,1)} %bitcast.13, bf16[2048,128]{1,0:T(8,128)(2,1)} %bitcast.15, bf16[128,2048]{1,0:T(8,128)(2,1)} %bitcast.17), custom_call_target="tpu_custom_call" | custom-call | tf_op jit(solution)/shard_map/pallas_call | solution.py:318
  20.0 0.0 copy-start.8
  20.0 1.1 copy-done.8
  21.1 9.5 %all-to-all-done = bf16[16,9,4,128]{3,2,1,0:T(4,128)(2,1)S(1)} async-done(((bf16[16,9,4,128]{3,2,1,0:T(4,128)(2,1)}), bf16[16,9,4,128]{3,2,1,0:T(4,128)(2,1)S(1)}, u32[]{:S(2)}, u32[]{:S(2)}) %all-to-all-start) | async-done | bytes 147488 | tf_op jit(solution)/shard_map/all_to_all | solution.py:293
  30.6 0.5 shard_map.112
  31.1 0.0 copy-start
  31.1 1.4 %copy-done = bf16[16,576,128]{2,1,0:T(8,128)(2,1)} copy-done((bf16[16,576,128]{2,1,0:T(8,128)(2,1)}, bf16[16,576,128]{2,1,0:T(8,128)(2,1)S(1)}, u32[]{:S(2)}) %copy-start) | copy-done | bytes 2359320
  32.5 6.8 %all-to-all-start.1 = ((bf16[16,576,128]{2,1,0:T(8,128)(2,1)}), bf16[16,576,128]{2,1,0:T(8,128)(2,1)S(1)}, u32[]{:S(2)}, u32[]{:S(2)}) async-start(bf16[16,576,128]{2,1,0:T(8,128)(2,1)} %copy-done), calls=%async_computation.1 | async-start | bytes 4718592 | tf_op jit(solution)/shard_map/all_to_all | solution.py:293
  39.3 0.0 copy-start.3
  39.3 0.0 copy-start.4
  39.3 6.4 %collective-permute-start = (bf16[6144,128]{1,0:T(8,128)(2,1)}, bf16[6144,128]{1,0:T(8,128)(2,1)S(1)}, u32[]{:S(2)}, u32[]{:S(2)}) collective-permute-start(bf16[6144,128]{1,0:T(8,128)(2,1)} %copy-done.8), channel_id=1, source_target_pairs={{0,16},{16,0},{1,17},{17,1},{2,18},{18,2},{3,19},{19,3},{4,20},{20... | collective-permute-start | bytes 4718600 | tf_op jit(solution)/shard_map/ppermute | solution.py:297
  45.7 3.2 %collective-permute-done.in_ref = bf16[6144,128]{1,0:T(8,128)(2,1)S(1)} collective-permute-done((bf16[6144,128]{1,0:T(8,128)(2,1)}, bf16[6144,128]{1,0:T(8,128)(2,1)S(1)}, u32[]{:S(2)}, u32[]{:S(2)}) %collective-permute-start) | collective-permute-done | bytes 1572896 | tf_op jit(solution)/shard_map/ppermute | solution.py:297
  48.9 0.0 copy-start.1
  48.9 1.1 copy-done.1
  50.1 16.9 %all-to-all-done.1.own_ref = bf16[16,576,128]{2,1,0:T(8,128)(2,1)S(1)} async-done(((bf16[16,576,128]{2,1,0:T(8,128)(2,1)}), bf16[16,576,128]{2,1,0:T(8,128)(2,1)S(1)}, u32[]{:S(2)}, u32[]{:S(2)}) %all-to-all-start.1) | async-done | bytes 2359328 | tf_op jit(solution)/shard_map/all_to_all | solution.py:293
  67.0 0.0 copy-done.3
  67.0 0.0 copy-done.4
  67.0 0.0 copy-start.2
  67.0 1.4 %copy-done.2 = bf16[6144,128]{1,0:T(8,128)(2,1)S(1)} copy-done((bf16[6144,128]{1,0:T(8,128)(2,1)S(1)}, bf16[6144,128]{1,0:T(8,128)(2,1)}, u32[]{:S(2)}) %copy-start.2) | copy-done | bytes 1572888
  68.4 0.0 copy-start.5
  68.4 1.0 copy-done.5
  69.4 2.4 %shard_map.114 = (bf16[16,296,128]{2,1,0:T(8,128)(2,1)S(1)}, bf16[288,512]{1,0:T(8,128)(2,1)S(1)}, bf16[288,256]{1,0:T(8,128)(2,1)S(1)}) custom-call(bf16[16,576,128]{2,1,0:T(8,128)(2,1)S(1)} %all-to-all-done.1.own_ref, bf16[2048,128]{1,0:T(8,128)(2,1)S(1)} %bitcast.14, bf16[2048,128]{1,0:T(8,128)(2,1)S(1)} %bitcast.16, bf16[128,2048]{1,0:T(8,128)(2,1)S(1)} %bitcast.18, ...), custom_call_target="tpu_custom_call" | custom-call | tf_op jit(solution)/shard_map/pallas_call | solution.py:337
  71.8 0.0 copy-start.6
  71.8 2.2 %shard_map.118 = bf16[384,2048]{1,0:T(8,128)(2,1)} custom-call(bf16[16,576,128]{2,1,0:T(8,128)(2,1)S(1)} %all-to-all-done.1.own_ref, bf16[288,512]{1,0:T(8,128)(2,1)S(1)} %get-tuple-element.24.both_ref, bf16[288,256]{1,0:T(8,128)(2,1)S(1)} %get-tuple-element.25.hidden_ref), custom_call_target="tpu_custom_call" | custom-call | tf_op jit(solution)/shard_map/pallas_call | solution.py:344
  74.1 0.0 copy-done.6
  74.1 8.8 %collective-permute-start.1 = (bf16[384,2048]{1,0:T(8,128)(2,1)}, bf16[384,2048]{1,0:T(8,128)(2,1)}, u32[]{:S(2)}, u32[]{:S(2)}) collective-permute-start(bf16[384,2048]{1,0:T(8,128)(2,1)} %shard_map.118), channel_id=1, source_target_pairs={{0,16},{16,0},{1,17},{17,1},{2,18},{18,2},{3,19},{19,3},{4,20},{20... | collective-permute-start | bytes 4718600 | tf_op jit(solution)/shard_map/ppermute | solution.py:297
  82.9 21.4 %all_to_all.20.in_ref = bf16[16,296,128]{2,1,0:T(8,128)(2,1)S(1)} all-to-all(bf16[16,296,128]{2,1,0:T(8,128)(2,1)S(1)} %get-tuple-element.19), channel_id=1, replica_groups=mesh['ep_0'=16,'ep_1'=2,'tp'=16] {'tp'}, dimensions={0} | all-to-all | bytes 2424832 | tf_op jit(solution)/shard_map/all_to_all | solution.py:293
  104.2 0.0 copy-start.7
  104.2 1.0 shard_map.115
  105.3 9.0 %all-to-all-start.3 = ((bf16[16,5,4,128]{3,2,1,0:T(4,128)(2,1)}), bf16[16,5,4,128]{3,2,1,0:T(4,128)(2,1)S(1)}, u32[]{:S(2)}, u32[]{:S(2)}) async-start(bf16[16,5,4,128]{3,2,1,0:T(4,128)(2,1)} %bitcast.7), calls=%async_computation.3 | async-start | bytes 163840 | tf_op jit(solution)/shard_map/all_to_all | solution.py:293
  114.3 1.2 shard_map.116
  115.5 10.6 %all-to-all-done.3 = bf16[16,5,4,128]{3,2,1,0:T(4,128)(2,1)S(1)} async-done(((bf16[16,5,4,128]{3,2,1,0:T(4,128)(2,1)}), bf16[16,5,4,128]{3,2,1,0:T(4,128)(2,1)S(1)}, u32[]{:S(2)}, u32[]{:S(2)}) %all-to-all-start.3) | async-done | bytes 81952 | tf_op jit(solution)/shard_map/all_to_all | solution.py:293
  126.1 1.0 shard_map.117
  127.2 0.0 collective-permute-done.1.other_ref
  127.2 0.0 copy-done.7
  127.2 3.6 %shard_map.119 = (bf16[2048,128]{1,0:T(8,128)(2,1)}, bf16[2048,128]{1,0:T(8,128)(2,1)}, bf16[128,2048]{1,0:T(8,128)(2,1)}) custom-call(bf16[16,576,128]{2,1,0:T(8,128)(2,1)S(1)} %all-to-all-done.1.own_ref, bf16[288,512]{1,0:T(8,128)(2,1)S(1)} %copy-done.7, bf16[288,256]{1,0:T(8,128)(2,1)S(1)} %get-tuple-element.25.hidden_ref, ...), custom_call_target="tpu_custom_call" | custom-call | tf_op jit(solution)/shard_map/pallas_call | solution.py:346
  (1 shorter events, 0.0 us)
Async XLA Ops:
  2.8 27.8 %all-to-all-start = ((bf16[16,9,4,128]{3,2,1,0:T(4,128)(2,1)}), bf16[16,9,4,128]{3,2,1,0:T(4,128)(2,1)S(1)}, u32[]{:S(2)}, u32[]{:S(2)}) async-start(bf16[16,9,4,128]{3,2,1,0:T(4,128)(2,1)} %bitcast.2), calls=%async_computation | async-start | bytes 294912 | tf_op jit(solution)/shard_map/all_to_all | solution.py:293
  20.0 1.1 copy-start.8
  31.1 1.4 %copy-start = (bf16[16,576,128]{2,1,0:T(8,128)(2,1)}, bf16[16,576,128]{2,1,0:T(8,128)(2,1)S(1)}, u32[]{:S(2)}) copy-start(bf16[16,576,128]{2,1,0:T(8,128)(2,1)S(1)} %shard_map.112) | copy-start | bytes 7077892
  32.5 34.4 %all-to-all-start.1 = ((bf16[16,576,128]{2,1,0:T(8,128)(2,1)}), bf16[16,576,128]{2,1,0:T(8,128)(2,1)S(1)}, u32[]{:S(2)}, u32[]{:S(2)}) async-start(bf16[16,576,128]{2,1,0:T(8,128)(2,1)} %copy-done), calls=%async_computation.1 | async-start | bytes 4718592 | tf_op jit(solution)/shard_map/all_to_all | solution.py:293
  39.3 27.7 %copy-start.3 = (bf16[1,2048,128]{2,1,0:T(8,128)(2,1)S(1)}, bf16[1,2048,128]{2,1,0:T(8,128)(2,1)}, u32[]{:S(2)}) copy-start(bf16[1,2048,128]{2,1,0:T(8,128)(2,1)} %param.11) | copy-start | bytes 1572868
  39.3 27.7 %copy-start.4 = (bf16[1,2048,128]{2,1,0:T(8,128)(2,1)S(1)}, bf16[1,2048,128]{2,1,0:T(8,128)(2,1)}, u32[]{:S(2)}) copy-start(bf16[1,2048,128]{2,1,0:T(8,128)(2,1)} %param.12) | copy-start | bytes 1572868
  39.3 9.6 %collective-permute-start = (bf16[6144,128]{1,0:T(8,128)(2,1)}, bf16[6144,128]{1,0:T(8,128)(2,1)S(1)}, u32[]{:S(2)}, u32[]{:S(2)}) collective-permute-start(bf16[6144,128]{1,0:T(8,128)(2,1)} %copy-done.8), channel_id=1, source_target_pairs={{0,16},{16,0},{1,17},{17,1},{2,18},{18,2},{3,19},{19,3},{4,20},{20... | collective-permute-start | bytes 4718600 | tf_op jit(solution)/shard_map/ppermute | solution.py:297
  48.9 1.1 copy-start.1
  67.0 1.4 %copy-start.2 = (bf16[6144,128]{1,0:T(8,128)(2,1)S(1)}, bf16[6144,128]{1,0:T(8,128)(2,1)}, u32[]{:S(2)}) copy-start(bf16[6144,128]{1,0:T(8,128)(2,1)} %shard_map.113.swap_ref) | copy-start | bytes 4718596
  68.4 1.0 copy-start.5
  71.8 2.2 %copy-start.6 = (bf16[288,512]{1,0:T(8,128)(2,1)}, bf16[288,512]{1,0:T(8,128)(2,1)S(1)}, u32[]{:S(2)}) copy-start(bf16[288,512]{1,0:T(8,128)(2,1)S(1)} %get-tuple-element.24.both_ref) | copy-start | bytes 884740
  74.1 53.1 %collective-permute-start.1 = (bf16[384,2048]{1,0:T(8,128)(2,1)}, bf16[384,2048]{1,0:T(8,128)(2,1)}, u32[]{:S(2)}, u32[]{:S(2)}) collective-permute-start(bf16[384,2048]{1,0:T(8,128)(2,1)} %shard_map.118), channel_id=1, source_target_pairs={{0,16},{16,0},{1,17},{17,1},{2,18},{18,2},{3,19},{19,3},{4,20},{20... | collective-permute-start | bytes 4718600 | tf_op jit(solution)/shard_map/ppermute | solution.py:297
  104.2 22.9 %copy-start.7 = (bf16[288,512]{1,0:T(8,128)(2,1)S(1)}, bf16[288,512]{1,0:T(8,128)(2,1)}, u32[]{:S(2)}) copy-start(bf16[288,512]{1,0:T(8,128)(2,1)} %copy-done.6) | copy-start | bytes 884740
  105.3 20.8 %all-to-all-start.3 = ((bf16[16,5,4,128]{3,2,1,0:T(4,128)(2,1)}), bf16[16,5,4,128]{3,2,1,0:T(4,128)(2,1)S(1)}, u32[]{:S(2)}, u32[]{:S(2)}) async-start(bf16[16,5,4,128]{3,2,1,0:T(4,128)(2,1)} %bitcast.7), calls=%async_computation.3 | async-start | bytes 163840 | tf_op jit(solution)/shard_map/all_to_all | solution.py:293

commit v6 on v5

--- a/solution.py
+++ b/solution.py
@@ -41,6 +41,16 @@
 
 def matmul(left, right):
     return lax.dot_general(left, right, (((1,), (0,)), ((), ())), preferred_element_type=F32)
+
+
+def member_at(place):
+    return jnp.where((place & 1) == 1, (9 + (place >> 1)) & 15, 8 - (place >> 1))
+
+
+def own_lanes():
+    z = lax.axis_index("ep_0")
+    place = jnp.where(z == 0, 15, jnp.where(z < 9, 16 - 2 * z, 2 * z - 17))
+    return (place % 4) * 32
 
 
 def expand(expert, values):
@@ -81,9 +91,10 @@
     weight = jnp.where(first, weights[0:1, :], 0.0) + jnp.where(second, weights[1:2, :], 0.0)
     slot = jnp.where(member > 0.0, rank, -100.0)
     row = iota((16 * PIECE, 1), 0)
-    expert = (row * 1821) >> 16
+    place = (row * 1821) >> 16
+    expert = member_at(place)
     slots = expand(expert, slot.astype(BF)).astype(jnp.int32)
-    within = row - expert * PIECE
+    within = row - place * PIECE
     sel_x = slots == within
     sel_dy = slots + CAP == within
     high, low = split_two(weight)
@@ -132,11 +143,12 @@
     first, second, member, rank = ranks(routes)
     slot = jnp.where(member > 0.0, rank, -100.0)
     row = iota((16 * BACK, 1), 0)
-    expert = (row * 3277) >> 16
-    within = row - expert * BACK
+    place = (row * 3277) >> 16
+    expert = member_at(place)
+    within = row - place * BACK
     sel = jnp.where(expand(expert, slot.astype(BF)).astype(jnp.int32) == within, 1.0, 0.0)
     combine_ref[0:128, :] = jnp.transpose(sel).astype(BF)
-    offset = (lax.axis_index("ep_0") % 4) * 32
+    offset = own_lanes()
     weights = weights_ref[...]
     for k, mine in enumerate((first, second)):
         sel = jnp.where(within >= CAP, expand(expert, one_if(mine)), 0.0)
@@ -290,7 +302,8 @@
 
 
 def exchange(value, axis):
-    return lax.all_to_all(value, axis, 0, 0, tiled=True)
+    groups = [[8 - k // 2 if k % 2 == 0 else (9 + k // 2) % 16 for k in range(16)]] if axis == "ep_0" else None
+    return lax.all_to_all(value, axis, 0, 0, axis_index_groups=groups, tiled=True)
 
 
 def to_partner(value):
@@ -333,7 +346,8 @@
     copies = kernel(copies_kernel, out_shape=near((16, GATH, 128)))(
         hold(received.reshape(SRC * PIECE, 128)), hold(pick_copies)
     )
-    own = hold(exchange(copies, "tp"))
+    gathered = exchange(copies, "tp")
+    own, own_far = hold(gathered), far(gathered)
     part, both, hidden = kernel(
         main_kernel,
         in_specs=[vmem] * 5,
@@ -341,11 +355,11 @@
         out_shape=(near((16, PART, 128)), near((ROWS, 512)), near((ROWS, 256))),
     )(own, gate, up, down, packed_2)
     spread = exchange(part, "tp")
-    partner = kernel(partner_grads_kernel, out_shape=shape((384, width)))(own, both, hidden)
+    partner = kernel(partner_grads_kernel, out_shape=shape((384, width)))(own_far, both, hidden)
     mine = to_partner(partner)
     gate_grad, up_grad, down_grad = kernel(
         own_grads_kernel, out_shape=(shape((width, 128)), shape((width, 128)), shape((128, width)))
-    )(own, both, hidden, mine)
+    )(own_far, both, hidden, mine)
     back = kernel(sum_kernel, out_shape=near((SRC * BACK, 128)))(hold(spread))
     pick_combine, lanes = kernel(
         places_kernel,

time: 132 us -> 130 us (0.985)
  waiting for transfers between devices: 40.2 us -> 35.1 us
  local copies, waits for them, and re-layouts: 6.16 us -> 10.3 us
  starting transfers between devices: 46.7 us -> 44.9 us
    ppermute x2, starting transfers between devices: 15.2 us -> 7.56 us  [to_partner(): return lax.ppermute(value, 'ep_1', [(0, 1), (1, 0)])]
    all_to_all x3, starting transfers between devices: 31.5 us -> 37.4 us  [exchange(): lax.all_to_all(value, axis, 0, 0, axis_index_groups=groups, tiled=True)]
    all_to_all x3, waiting for transfers between devices: 37 us -> 31.8 us  [exchange(): lax.all_to_all(value, axis, 0, 0, axis_index_groups=groups, tiled=True)]
    unnamed x18 -> x32, local copies, waits for them, and re-layouts: 6.16 us -> 10.3 us
where the time goes in v6:
time: 130 us; the launch traced here: 129 us
  starting transfers between devices  44.9 us (35%)
  waiting for transfers between devices  35.1 us (27%)
  blocking collectives  21.6 us (17%)
  Pallas kernels  16.5 us (13%)
  local copies, waits for them, and re-layouts  10.3 us (8%)
    all_to_all x3, starting transfers between devices, exchange(): lax.all_to_all(value, axis, 0, 0, axis_index_groups=groups, tiled=True)  37.4 us
    all_to_all x3, waiting for transfers between devices, exchange(): lax.all_to_all(value, axis, 0, 0, axis_index_groups=groups, tiled=True)  31.8 us
    all_to_all x1, blocking collectives, exchange(): lax.all_to_all(value, axis, 0, 0, axis_index_groups=groups, tiled=True)  21.6 us
    unnamed x32, local copies, waits for them, and re-layouts  10.3 us
    ppermute x2, starting transfers between devices, to_partner(): return lax.ppermute(value, 'ep_1', [(0, 1), (1, 0)])  7.56 us
    pallas_call x1, Pallas kernels, steps(): kernel(own_grads_kernel, out_shape=(shape((width, 128)), shape((width, 12...  3.86 us
    ppermute x2, waiting for transfers between devices, to_partner(): return lax.ppermute(value, 'ep_1', [(0, 1), (1, 0)])  3.23 us
    pallas_call x1, Pallas kernels, steps(): kernel(partner_grads_kernel, out_shape=shape((384, width)))  2.86 us
  transfers between devices with their start and end apart: 5, of which 4 were waited for; matrix products, arithmetic and copies ran while one was open for 0% of the time, Pallas kernels for 4%

profile of v6, /device:TPU:1, one launch (start us, length us, event | category | flops | bytes accessed | tf_op | source)
XLA Modules:
  0.0 129.2 jit_solution(5213881983047626020)
XLA Ops:
  0.6 2.2 %shard_map.110 = bf16[576,128]{1,0:T(8,128)(2,1)} custom-call(s32[2,128]{1,0:T(2,128)} %bitcast.21, f32[2,128]{1,0:T(2,128)} %bitcast.23, bf16[128,2048]{1,0:T(8,128)(2,1)} %tokens_ref.1, bf16[128,2048]{1,0:T(8,128)(2,1)} %grad_ref.1), custom_call_target="tpu_custom_call" | custom-call | tf_op jit(solution)/shard_map/pallas_call | solution.py:324
  2.8 19.1 %all-to-all-start = ((bf16[16,9,4,128]{3,2,1,0:T(4,128)(2,1)}), bf16[16,9,4,128]{3,2,1,0:T(4,128)(2,1)S(1)}, u32[]{:S(2)}, u32[]{:S(2)}) async-start(bf16[16,9,4,128]{3,2,1,0:T(4,128)(2,1)} %bitcast.2), calls=%async_computation | async-start | bytes 294912 | tf_op jit(solution)/shard_map/all_to_all | solution.py:306
  22.0 1.4 %shard_map.111 = (bf16[576,576]{1,0:T(8,128)(2,1)S(1)}, bf16[6144,128]{1,0:T(8,128)(2,1)S(1)}) custom-call(bf16[2048,128]{1,0:T(8,128)(2,1)} %bitcast.13, bf16[2048,128]{1,0:T(8,128)(2,1)} %bitcast.15, bf16[128,2048]{1,0:T(8,128)(2,1)} %bitcast.17), custom_call_target="tpu_custom_call" | custom-call | tf_op jit(solution)/shard_map/pallas_call | solution.py:331
  23.4 0.0 copy-start.15
  23.4 1.1 copy-done.15
  24.5 4.9 %all-to-all-done = bf16[16,9,4,128]{3,2,1,0:T(4,128)(2,1)S(1)} async-done(((bf16[16,9,4,128]{3,2,1,0:T(4,128)(2,1)}), bf16[16,9,4,128]{3,2,1,0:T(4,128)(2,1)S(1)}, u32[]{:S(2)}, u32[]{:S(2)}) %all-to-all-start) | async-done | bytes 147488 | tf_op jit(solution)/shard_map/all_to_all | solution.py:306
  29.4 0.5 shard_map.112
  29.9 0.0 copy-start.1
  29.9 1.4 %copy-done.1 = bf16[16,576,128]{2,1,0:T(8,128)(2,1)} copy-done((bf16[16,576,128]{2,1,0:T(8,128)(2,1)}, bf16[16,576,128]{2,1,0:T(8,128)(2,1)S(1)}, u32[]{:S(2)}) %copy-start.1) | copy-done | bytes 2359320
  31.4 6.8 %all-to-all-start.1 = ((bf16[16,576,128]{2,1,0:T(8,128)(2,1)}), bf16[16,576,128]{2,1,0:T(8,128)(2,1)S(1)}, u32[]{:S(2)}, u32[]{:S(2)}) async-start(bf16[16,576,128]{2,1,0:T(8,128)(2,1)} %copy-done.1), calls=%async_computation.1 | async-start | bytes 4718592 | tf_op jit(solution)/shard_map/all_to_all | solution.py:306
  38.1 0.0 copy-start.4
  38.1 0.0 copy-start.5
  38.2 3.3 %collective-permute-start = (bf16[6144,128]{1,0:T(8,128)(2,1)}, bf16[6144,128]{1,0:T(8,128)(2,1)S(1)}, u32[]{:S(2)}, u32[]{:S(2)}) collective-permute-start(bf16[6144,128]{1,0:T(8,128)(2,1)} %copy-done.15), channel_id=1, source_target_pairs={{0,16},{16,0},{1,17},{17,1},{2,18},{18,2},{3,19},{19,3},{4,20},{20... | collective-permute-start | bytes 4718600 | tf_op jit(solution)/shard_map/ppermute | solution.py:310
  41.5 3.2 %collective-permute-done.in_ref = bf16[6144,128]{1,0:T(8,128)(2,1)S(1)} collective-permute-done((bf16[6144,128]{1,0:T(8,128)(2,1)}, bf16[6144,128]{1,0:T(8,128)(2,1)S(1)}, u32[]{:S(2)}, u32[]{:S(2)}) %collective-permute-start) | collective-permute-done | bytes 1572896 | tf_op jit(solution)/shard_map/ppermute | solution.py:310
  44.7 0.0 copy-start.2
  44.7 1.2 copy-done.2
  45.8 26.0 %all-to-all-done.1.own_ref = bf16[16,576,128]{2,1,0:T(8,128)(2,1)S(1)} async-done(((bf16[16,576,128]{2,1,0:T(8,128)(2,1)}), bf16[16,576,128]{2,1,0:T(8,128)(2,1)S(1)}, u32[]{:S(2)}, u32[]{:S(2)}) %all-to-all-start.1) | async-done | bytes 2359328 | tf_op jit(solution)/shard_map/all_to_all | solution.py:306
  71.9 0.0 copy-done.4
  71.9 0.0 copy-done.5
  71.9 0.0 copy-start.3
  71.9 1.4 %copy-done.3 = bf16[6144,128]{1,0:T(8,128)(2,1)S(1)} copy-done((bf16[6144,128]{1,0:T(8,128)(2,1)S(1)}, bf16[6144,128]{1,0:T(8,128)(2,1)}, u32[]{:S(2)}) %copy-start.3) | copy-done | bytes 1572888
  73.3 0.0 copy-start.6
  73.3 1.0 copy-done.6
  74.3 0.0 copy-start
  74.3 2.4 %shard_map.114 = (bf16[16,296,128]{2,1,0:T(8,128)(2,1)S(1)}, bf16[288,512]{1,0:T(8,128)(2,1)S(1)}, bf16[288,256]{1,0:T(8,128)(2,1)S(1)}) custom-call(bf16[16,576,128]{2,1,0:T(8,128)(2,1)S(1)} %all-to-all-done.1.own_ref, bf16[2048,128]{1,0:T(8,128)(2,1)S(1)} %bitcast.14, bf16[2048,128]{1,0:T(8,128)(2,1)S(1)} %bitcast.16, bf16[128,2048]{1,0:T(8,128)(2,1)S(1)} %bitcast.18, ...), custom_call_target="tpu_custom_call" | custom-call | tf_op jit(solution)/shard_map/pallas_call | solution.py:351
  76.7 0.0 copy-done
  76.8 0.0 copy-start.7
  76.8 0.0 copy-start.9
  76.8 2.9 %shard_map.118 = bf16[384,2048]{1,0:T(8,128)(2,1)S(1)} custom-call(bf16[16,576,128]{2,1,0:T(8,128)(2,1)} %copy-done, bf16[288,512]{1,0:T(8,128)(2,1)S(1)} %get-tuple-element.24.both_ref, bf16[288,256]{1,0:T(8,128)(2,1)S(1)} %get-tuple-element.25.hidden_ref), custom_call_target="tpu_custom_call" | custom-call | tf_op jit(solution)/shard_map/pallas_call | solution.py:358
  79.6 0.0 copy-done.7
  79.7 0.0 copy-done.9
  79.7 4.3 %collective-permute-start.1 = (bf16[384,2048]{1,0:T(8,128)(2,1)S(1)}, bf16[384,2048]{1,0:T(8,128)(2,1)S(1)}, u32[]{:S(2)}, u32[]{:S(2)}) collective-permute-start(bf16[384,2048]{1,0:T(8,128)(2,1)S(1)} %shard_map.118), channel_id=1, source_target_pairs={{0,16},{16,0},{1,17},{17,1},{2,18},{18,2},{3,19},{19,3},{4,20},{20... | collective-permute-start | bytes 4718600 | tf_op jit(solution)/shard_map/ppermute | solution.py:310
  83.9 21.6 %all_to_all.20.in_ref = bf16[16,296,128]{2,1,0:T(8,128)(2,1)S(1)} all-to-all(bf16[16,296,128]{2,1,0:T(8,128)(2,1)S(1)} %get-tuple-element.19), channel_id=1, replica_groups=mesh['ep_0'=16,'ep_1'=2,'tp'=16] {'tp'}, dimensions={0} | all-to-all | bytes 2424832 | tf_op jit(solution)/shard_map/all_to_all | solution.py:306
  105.6 0.0 copy-start.8
  105.6 1.0 shard_map.115
  106.6 11.5 %all-to-all-start.3 = ((bf16[16,5,4,128]{3,2,1,0:T(4,128)(2,1)}), bf16[16,5,4,128]{3,2,1,0:T(4,128)(2,1)S(1)}, u32[]{:S(2)}, u32[]{:S(2)}) async-start(bf16[16,5,4,128]{3,2,1,0:T(4,128)(2,1)} %bitcast.7), calls=%async_computation.3 | async-start | bytes 163840 | tf_op jit(solution)/shard_map/all_to_all | solution.py:306
  118.1 1.2 shard_map.116
  119.3 0.0 copy-start.11
  119.3 0.7 copy-done.11
  120.0 0.0 copy-start.13
  120.0 0.6 copy-done.13
  120.6 0.9 all-to-all-done.3
  121.5 0.0 copy-start.12
  121.5 1.0 copy-done.12
  122.5 0.0 copy-start.14
  122.5 0.9 copy-done.14
  123.4 1.0 shard_map.117
  124.4 0.0 collective-permute-done.1.other_ref
  124.5 0.0 copy-done.8
  124.5 0.0 copy-start.10
  124.5 0.9 copy-done.10
  125.4 3.9 %shard_map.119 = (bf16[2048,128]{1,0:T(8,128)(2,1)}, bf16[2048,128]{1,0:T(8,128)(2,1)}, bf16[128,2048]{1,0:T(8,128)(2,1)}) custom-call(bf16[16,576,128]{2,1,0:T(8,128)(2,1)} %copy-done, bf16[288,512]{1,0:T(8,128)(2,1)S(1)} %copy-done.8, bf16[288,256]{1,0:T(8,128)(2,1)S(1)} %copy-done.10, bf16[384,2048]{1,0:T(8,128)(2,1)S(1)} %collective-permute-done.1.other_ref), custom_call_target="tpu_custom_call" | custom-call | tf_op jit(solution)/shard_map/pallas_call | solution.py:360
  (1 shorter events, 0.0 us)
Async XLA Ops:
  2.8 26.6 %all-to-all-start = ((bf16[16,9,4,128]{3,2,1,0:T(4,128)(2,1)}), bf16[16,9,4,128]{3,2,1,0:T(4,128)(2,1)S(1)}, u32[]{:S(2)}, u32[]{:S(2)}) async-start(bf16[16,9,4,128]{3,2,1,0:T(4,128)(2,1)} %bitcast.2), calls=%async_computation | async-start | bytes 294912 | tf_op jit(solution)/shard_map/all_to_all | solution.py:306
  23.4 1.2 copy-start.15
  29.9 1.4 %copy-start.1 = (bf16[16,576,128]{2,1,0:T(8,128)(2,1)}, bf16[16,576,128]{2,1,0:T(8,128)(2,1)S(1)}, u32[]{:S(2)}) copy-start(bf16[16,576,128]{2,1,0:T(8,128)(2,1)S(1)} %shard_map.112) | copy-start | bytes 7077892
  31.4 40.5 %all-to-all-start.1 = ((bf16[16,576,128]{2,1,0:T(8,128)(2,1)}), bf16[16,576,128]{2,1,0:T(8,128)(2,1)S(1)}, u32[]{:S(2)}, u32[]{:S(2)}) async-start(bf16[16,576,128]{2,1,0:T(8,128)(2,1)} %copy-done.1), calls=%async_computation.1 | async-start | bytes 4718592 | tf_op jit(solution)/shard_map/all_to_all | solution.py:306
  38.1 33.8 %copy-start.4 = (bf16[1,2048,128]{2,1,0:T(8,128)(2,1)S(1)}, bf16[1,2048,128]{2,1,0:T(8,128)(2,1)}, u32[]{:S(2)}) copy-start(bf16[1,2048,128]{2,1,0:T(8,128)(2,1)} %param.11) | copy-start | bytes 1572868
  38.1 33.7 %copy-start.5 = (bf16[1,2048,128]{2,1,0:T(8,128)(2,1)S(1)}, bf16[1,2048,128]{2,1,0:T(8,128)(2,1)}, u32[]{:S(2)}) copy-start(bf16[1,2048,128]{2,1,0:T(8,128)(2,1)} %param.12) | copy-start | bytes 1572868
  38.2 6.5 %collective-permute-start = (bf16[6144,128]{1,0:T(8,128)(2,1)}, bf16[6144,128]{1,0:T(8,128)(2,1)S(1)}, u32[]{:S(2)}, u32[]{:S(2)}) collective-permute-start(bf16[6144,128]{1,0:T(8,128)(2,1)} %copy-done.15), channel_id=1, source_target_pairs={{0,16},{16,0},{1,17},{17,1},{2,18},{18,2},{3,19},{19,3},{4,20},{20... | collective-permute-start | bytes 4718600 | tf_op jit(solution)/shard_map/ppermute | solution.py:310
  44.7 1.2 copy-start.2
  71.9 1.4 %copy-start.3 = (bf16[6144,128]{1,0:T(8,128)(2,1)S(1)}, bf16[6144,128]{1,0:T(8,128)(2,1)}, u32[]{:S(2)}) copy-start(bf16[6144,128]{1,0:T(8,128)(2,1)} %shard_map.113.swap_ref) | copy-start | bytes 4718596
  73.3 1.0 copy-start.6
  74.3 2.4 %copy-start = (bf16[16,576,128]{2,1,0:T(8,128)(2,1)}, bf16[16,576,128]{2,1,0:T(8,128)(2,1)S(1)}, u32[]{:S(2)}) copy-start(bf16[16,576,128]{2,1,0:T(8,128)(2,1)S(1)} %all-to-all-done.1.own_ref) | copy-start | bytes 7077892
  76.8 2.9 %copy-start.7 = (bf16[288,512]{1,0:T(8,128)(2,1)}, bf16[288,512]{1,0:T(8,128)(2,1)S(1)}, u32[]{:S(2)}) copy-start(bf16[288,512]{1,0:T(8,128)(2,1)S(1)} %get-tuple-element.24.both_ref) | copy-start | bytes 884740
  76.8 2.9 %copy-start.9 = (bf16[288,256]{1,0:T(8,128)(2,1)}, bf16[288,256]{1,0:T(8,128)(2,1)S(1)}, u32[]{:S(2)}) copy-start(bf16[288,256]{1,0:T(8,128)(2,1)S(1)} %get-tuple-element.25.hidden_ref) | copy-start | bytes 442372
  79.7 44.8 %collective-permute-start.1 = (bf16[384,2048]{1,0:T(8,128)(2,1)S(1)}, bf16[384,2048]{1,0:T(8,128)(2,1)S(1)}, u32[]{:S(2)}, u32[]{:S(2)}) collective-permute-start(bf16[384,2048]{1,0:T(8,128)(2,1)S(1)} %shard_map.118), channel_id=1, source_target_pairs={{0,16},{16,0},{1,17},{17,1},{2,18},{18,2},{3,19},{19,3},{4,20},{20... | collective-permute-start | bytes 4718600 | tf_op jit(solution)/shard_map/ppermute | solution.py:310
  105.6 18.9 %copy-start.8 = (bf16[288,512]{1,0:T(8,128)(2,1)S(1)}, bf16[288,512]{1,0:T(8,128)(2,1)}, u32[]{:S(2)}) copy-start(bf16[288,512]{1,0:T(8,128)(2,1)} %copy-done.7) | copy-start | bytes 884740
  106.6 15.0 %all-to-all-start.3 = ((bf16[16,5,4,128]{3,2,1,0:T(4,128)(2,1)}), bf16[16,5,4,128]{3,2,1,0:T(4,128)(2,1)S(1)}, u32[]{:S(2)}, u32[]{:S(2)}) async-start(bf16[16,5,4,128]{3,2,1,0:T(4,128)(2,1)} %bitcast.7), calls=%async_computation.3 | async-start | bytes 163840 | tf_op jit(solution)/shard_map/all_to_all | solution.py:306
  119.3 0.7 copy-start.11
  120.0 0.6 copy-start.13
  121.5 1.0 copy-start.12
  122.5 0.9 copy-start.14
  124.5 0.9 copy-start.10
